TPU v7x, 32 devices: a whole 2x2x4 slice. The times are simulated.
32 devices in a mesh: sp: 16 (over z, y, x), tp: 2 (over core).
Axes of the slice: x: 2, y: 2, z: 4, core: 2. Of those that a mesh axis runs over, the one named last changes fastest.
Arguments:
- conv_in: bfloat16 [4096, 1024], P('sp', 'tp'), may hold values from -6 to 6
- gate_outer: bfloat16 [4096, 1024], P('sp', 'tp'), may hold values from -6 to 6
- gate_inner: bfloat16 [4096, 1024], P('sp', 'tp'), may hold values from -6 to 6
- tap_weights: float32 [3, 1024], P(None, 'tp'), may hold values from -3 to 3
- doc_ids: int32 [4096], P('sp'), may hold values from 0 to 7, never falling along the last dimension, each value on 1 to 1024 neighbouring positions
- w_proj: bfloat16 [1024, 2048], replicated, may hold values from -0.1875 to 0.1875
- stream: bfloat16 [4096, 2048], P(('sp', 'tp')), may hold values from -6 to 6
- norm_gain: float32 [2048], replicated, may hold values from 0.1 to 1.9
- routes: int32 [4096, 4], P(('sp', 'tp')), may hold values from 0 to 31, all different within a row; in each aligned block of 128 rows (0 to 127, 128 to 255, ...) at most 32 rows name the same one
- route_weights: float32 [4096, 4], P(('sp', 'tp')), may hold values from 0.1 to 1
- w_gate: bfloat16 [32, 2048, 768], P(('sp', 'tp')), may hold values from -0.5 to 0.5
- w_up: bfloat16 [32, 2048, 768], P(('sp', 'tp')), may hold values from -0.5 to 0.5
- w_down: bfloat16 [32, 768, 2048], P(('sp', 'tp')), may hold values from -0.0546875 to 0.0546875
Outputs:
- layer_out: bfloat16 [4096, 2048], P(('sp', 'tp'))
Inputs may be any that keep to these rules, and one draw needn't show every extreme that they name: `doc_ids`: document numbers never fall along the sequence; a document covers at most 1024 positions. `routes`: a token names 4 different experts; among the rows of one device (aligned blocks of 128 tokens) no expert is named more than 32 times, a bound that some block reaches.
All inputs are finite; a program needn't handle non-finite values.
Results may differ from a plain program's by a relative error of at most 0.0071.
Values may be sent and summed in bfloat16 or wider, within the bound.
A program may use at most 128 MiB of HBM per device.

v0:
```python
import functools
import math

import jax
import jax.numpy as jnp
from jax import lax
from jax.experimental import pallas as pl
from jax.experimental.pallas import tpu as pltpu
from jax.sharding import PartitionSpec as P

MESH = pl.DeviceIdType.MESH


def with_halo(shard, sides, width):
    for axis, dim in sides:
        size, length = (lax.axis_size(axis), shard.shape[dim])
        up = [(i, (i + 1) % size) for i in range(size - 1)]
        down = [(j, i) for i, j in up]
        last = lax.slice_in_dim(shard, length - width, length, axis=dim)
        initial = lax.slice_in_dim(shard, 0, width, axis=dim)
        before = lax.ppermute(last, axis, up)
        after = lax.ppermute(initial, axis, down)
        shard = jnp.concatenate([before, shard, after], axis=dim)
    return shard


def dot(a, b):
    return jnp.dot(a, b, preferred_element_type=jnp.float32)


def tile_of(size, most):
    return next(t for t in range(most, 0, -128) if size % t == 0)


def schedule(steps):
    order, d, f, c = [], 0, 0, 0
    while c < steps:
        while d < steps and d < f + 2:
            order.append(("d", d))
            d += 1
        if f < steps:
            order.append(("f", f))
            f += 1
        if f - c >= 2 or f == steps:
            order.append(("c", c))
            c += 1
    return order


def moe_kernel(
    nz, n_plane, n_core, cap,
    normed, hidden, select, spread, wg_hbm, wu_hbm, wd_hbm,
    out_ref,
    wg, wu, wd, zbuf, outgoing, arrived, act, results, returned, partial, summed,
    w_sem, z_send, z_recv, a_send, a_recv, r_send, r_recv, p_send, p_recv,
):
    peers = n_plane * n_core
    width = normed.shape[1]
    rows = peers * cap
    ff = wg.shape[1]
    me = lax.axis_index("sp")
    core = lax.axis_index("tp")
    z, p = me // n_plane, lax.rem(me, n_plane)
    rank = p * n_core + core

    def z_peer(k):
        return {"sp": lax.rem(z + k, nz) * n_plane + p, "tp": core}

    def plane_peer(j):
        q = lax.rem(rank + j, peers)
        return {"sp": z * n_plane + q // n_core, "tp": lax.rem(q, n_core)}

    loads = [
        pltpu.make_async_copy(src, dst, w_sem.at[i])
        for i, (src, dst) in enumerate(((wg_hbm, wg), (wu_hbm, wu), (wd_hbm, wd)))
    ]
    for load in loads:
        load.start()
    barrier = pltpu.get_barrier_semaphore()
    for k in range(1, nz):
        pl.semaphore_signal(barrier, inc=1, device_id=z_peer(k), device_id_type=MESH)
    for j in range(1, peers):
        pl.semaphore_signal(barrier, inc=1, device_id=plane_peer(j), device_id_type=MESH)
    pl.semaphore_wait(barrier, nz - 1 + peers - 1)

    def remote(src, dst, send, recv, to):
        return pltpu.make_async_remote_copy(
            src_ref=src, dst_ref=dst, send_sem=send, recv_sem=recv,
            device_id=to, device_id_type=MESH)

    z_copies = {}
    for k in range(1, nz):
        z_copies[k] = remote(normed, zbuf.at[k - 1], z_send.at[k], z_recv.at[k], z_peer(k))
        z_copies[k].start()

    a_copies, r_copies, p_copies = {}, {}, {}
    col = tile_of(width, 512)
    fcol = tile_of(ff, 256)

    def dispatch(k):
        if k:
            z_copies[k].wait_recv()
        block = normed if k == 0 else zbuf.at[k - 1]

        @pl.loop(0, width // col)
        def _(i):
            cols = pl.ds(pl.multiple_of(i * col, col), col)
            picked = dot(select[k], block[:, cols]).astype(jnp.bfloat16)
            arrived[k, 0:cap, cols] = picked[:cap]
            outgoing[k, :, cols] = picked[cap:]

        for j in range(1, peers):
            a_copies[k, j] = remote(
                outgoing.at[k, pl.ds((j - 1) * cap, cap)], arrived.at[k, pl.ds(j * cap, cap)],
                a_send.at[k, j], a_recv.at[k, j], plane_peer(j))
            a_copies[k, j].start()

    def expert(k):
        if k == 0:
            for load in loads:
                load.wait()
        for j in range(1, peers):
            a_copies[k, j].wait_recv()

        @pl.loop(0, ff // fcol)
        def _(i):
            cols = pl.ds(pl.multiple_of(i * fcol, fcol), fcol)
            gate = jnp.minimum(dot(arrived[k], wg[:, cols]), 7.0)
            upper = jnp.clip(dot(arrived[k], wu[:, cols]), -7.0, 7.0)
            act[:, cols] = ((upper + 1.0) * gate * jax.nn.sigmoid(1.702 * gate)).astype(jnp.bfloat16)

        @pl.loop(0, width // col)
        def _(i):
            cols = pl.ds(pl.multiple_of(i * col, col), col)
            res = dot(act[...], wd[:, cols]).astype(jnp.bfloat16)
            returned[k, 0:cap, cols] = res[:cap]
            results[k, :, cols] = res[cap:]

        for j in range(1, peers):
            r_copies[k, j] = remote(
                results.at[k, pl.ds((j - 1) * cap, cap)], returned.at[k, pl.ds(j * cap, cap)],
                r_send.at[k, j], r_recv.at[k, j], plane_peer(peers - j))
            r_copies[k, j].start()

    def combine(k):
        for j in range(1, peers):
            r_copies[k, j].wait_recv()

        @pl.loop(0, width // col)
        def _(i):
            cols = pl.ds(pl.multiple_of(i * col, col), col)
            total = dot(spread[k], returned[k, :, cols])
            if k == 0:
                hidden[:, cols] = hidden[:, cols] + total
            else:
                partial[k - 1, :, cols] = total.astype(jnp.bfloat16)

        if k:
            p_copies[k] = remote(
                partial.at[k - 1], summed.at[k - 1], p_send.at[k], p_recv.at[k], z_peer(nz - k))
            p_copies[k].start()

    for kind, k in schedule(nz):
        {"d": dispatch, "f": expert, "c": combine}[kind](k)

    for k in range(1, nz):
        p_copies[k].wait_recv()

    @pl.loop(0, width // col)
    def _(i):
        cols = pl.ds(pl.multiple_of(i * col, col), col)
        total = hidden[:, cols]
        for k in range(1, nz):
            total = total + summed[k - 1, :, cols].astype(jnp.float32)
        out_ref[:, cols] = total.astype(jnp.bfloat16)

    for k in range(1, nz):
        z_copies[k].wait_send()
        p_copies[k].wait_send()
    for k in range(nz):
        for j in range(1, peers):
            a_copies[k, j].wait_send()
            r_copies[k, j].wait_send()


def moe(nz, n_plane, n_core, cap, normed, hidden, select, spread, wg, wu, wd):
    block, width = normed.shape
    ff = wg.shape[1]
    peers = n_plane * n_core
    rows = peers * cap
    bf = jnp.bfloat16
    vmem = pl.BlockSpec(memory_space=pltpu.VMEM)
    hbm = pl.BlockSpec(memory_space=pl.ANY)
    dma = pltpu.SemaphoreType.DMA

    def body(normed, hidden_in, *rest):
        hidden = rest[-1]
        hidden[...] = hidden_in[...]
        moe_kernel(nz, n_plane, n_core, cap, normed, hidden, *rest[:-1])

    return pl.pallas_call(
        body,
        out_shape=jax.ShapeDtypeStruct((block, width), bf),
        in_specs=[vmem] * 4 + [hbm] * 3,
        out_specs=vmem,
        scratch_shapes=[
            pltpu.VMEM((width, ff), bf),
            pltpu.VMEM((width, ff), bf),
            pltpu.VMEM((ff, width), bf),
            pltpu.VMEM((nz - 1, block, width), bf),
            pltpu.VMEM((nz, rows - cap, width), bf),
            pltpu.VMEM((nz, rows, width), bf),
            pltpu.VMEM((rows, ff), bf),
            pltpu.VMEM((nz, rows - cap, width), bf),
            pltpu.VMEM((nz, rows, width), bf),
            pltpu.VMEM((nz - 1, block, width), bf),
            pltpu.VMEM((nz - 1, block, width), bf),
            dma((3,)), dma((nz,)), dma((nz,)),
            dma((nz, peers)), dma((nz, peers)), dma((nz, peers)), dma((nz, peers)),
            dma((nz,)), dma((nz,)),
            pltpu.VMEM((block, width), jnp.float32),
        ],
        compiler_params=pltpu.CompilerParams(
            collective_id=0, has_side_effects=True, vmem_limit_bytes=60 * 2**20),
        name="moe_exchange",
    )(normed, hidden, select, spread, wg, wu, wd)


def slot_matrices(nz, n_plane, n_core, cap, routes, route_weights):
    block, topk = routes.shape
    peers = n_plane * n_core
    me = lax.axis_index("sp")
    z, p = me // n_plane, lax.rem(me, n_plane)
    rank = p * n_core + lax.axis_index("tp")
    groups = [[a * n_plane + b for a in range(nz)] for b in range(n_plane)]
    packed = jnp.concatenate([routes.astype(jnp.float32), route_weights], axis=1)
    every = lax.all_gather(packed, "sp", axis_index_groups=groups)
    every = every[(z - jnp.arange(nz)) % nz]
    chosen, weight = every[..., :topk].astype(jnp.int32), every[..., topk:]
    experts = z * peers + (rank + jnp.arange(peers)) % peers
    hit = chosen[..., None] == experts
    named = jnp.any(hit, axis=2)
    share = jnp.sum(jnp.where(hit, weight[..., None], 0.0), axis=2)
    below = jnp.tril(jnp.ones((block, block), jnp.bfloat16), -1)
    slot = jnp.einsum("ts,kse->kte", below, named.astype(jnp.bfloat16), preferred_element_type=jnp.float32)
    slot = jnp.where(named, slot.astype(jnp.int32), -1)
    place = slot[..., None] == jnp.arange(cap, dtype=jnp.int32)
    spread = jnp.where(place, share[..., None], 0.0).astype(jnp.bfloat16).reshape(nz, block, peers * cap)
    slot_t = jnp.swapaxes(slot, 1, 2)
    select = (slot_t[:, :, None, :] == jnp.arange(cap, dtype=jnp.int32)[:, None]).astype(jnp.bfloat16)
    return select.reshape(nz, peers * cap, block), spread


def per_device(
    conv_in,
    gate_outer,
    gate_inner,
    tap_weights,
    doc_ids,
    w_proj,
    stream,
    norm_gain,
    routes,
    route_weights,
    w_gate,
    w_up,
    w_down,
):
    n_seq = lax.axis_size("sp")
    n_core = lax.axis_size("tp")
    tok_dev = conv_in.shape[0]
    topk = routes.shape[1]
    n_expert = n_seq * n_core
    capacity = max(2, 2 * tok_dev * topk // (n_core * n_expert))
    capacity = -(-capacity // 16) * 16
    nz = max(d for d in range(1, math.isqrt(n_seq) + 1) if n_seq % d == 0)
    n_plane = n_seq // nz
    select, spread = slot_matrices(nz, n_plane, n_core, capacity, routes, route_weights)
    product = gate_inner.astype(jnp.float32) * conv_in.astype(jnp.float32)
    doc_float = doc_ids.astype(jnp.float32)
    wide_prod, wide_docs = (
        with_halo(product, (("sp", 0),), 1),
        with_halo(doc_float, (("sp", 0),), 1),
    )
    same_before = (wide_docs[1:-1] == wide_docs[:-2]).astype(jnp.float32)
    same_after = (wide_docs[1:-1] == wide_docs[2:]).astype(jnp.float32)
    conv = (
        tap_weights[0] * wide_prod[:-2] * same_before[:, None]
        + tap_weights[1] * product
        + tap_weights[2] * wide_prod[2:] * same_after[:, None]
    )
    mixed = (gate_outer.astype(jnp.float32) * conv).astype(jnp.bfloat16)
    regrouped = lax.all_to_all(mixed, "tp", split_axis=0, concat_axis=1, tiled=True)
    projected = jnp.dot(regrouped, w_proj, preferred_element_type=jnp.float32)
    hidden = stream.astype(jnp.float32) + projected
    scale = lax.rsqrt(jnp.mean(hidden * hidden, axis=-1, keepdims=True) + 1e-05)
    normed = (hidden * scale * norm_gain).astype(jnp.bfloat16)
    return moe(nz, n_plane, n_core, capacity, normed, hidden, select, spread, w_gate[0], w_up[0], w_down[0])


def solution(mesh):
    in_specs = (
        P("sp", "tp"),
        P("sp", "tp"),
        P("sp", "tp"),
        P(None, "tp"),
        P("sp"),
        P(),
        P(("sp", "tp"), None),
        P(),
        P(("sp", "tp"), None),
        P(("sp", "tp"), None),
        P(("sp", "tp"), None, None),
        P(("sp", "tp"), None, None),
        P(("sp", "tp"), None, None),
    )
    out_specs = P(("sp", "tp"), None)
    return jax.shard_map(
        per_device, mesh=mesh, in_specs=in_specs, out_specs=out_specs, check_vma=False
    )
```

profile of v0, /device:TPU:0, one launch (start us, length us, event | category | flops | bytes accessed | tf_op | source)
XLA Modules:
  0.0 182.4 jit_solution(10464259832589240239)
XLA Ops:
  0.0 0.8 convert_element_type.53
  0.8 0.6 fusion.25
  1.3 5.4 %collective-permute-start.1 = (f32[1]{0:T(128)}, f32[1]{0:T(128)}, u32[]{:S(2)}, u32[]{:S(2)}) collective-permute-start(f32[1]{0:T(128)} %get-tuple-element.16), channel_id=1, source_target_pairs={{0,2},{2,4},{4,6},{6,8},{8,10},{10,12},{12,14},{14,16},{16,18},{18... | collective-permute-start | bytes 20 | tf_op jit(solution)/shard_map/ppermute | solution.py:21
  6.8 1.3 collective-permute-start.3
  8.1 1.1 convert_multiply_fusion
  9.2 4.5 %collective-permute-start = (f32[1,512]{1,0:T(1,128)S(1)}, f32[1,512]{1,0:T(1,128)S(1)}, u32[]{:S(2)}, u32[]{:S(2)}) collective-permute-start(f32[1,512]{1,0:T(1,128)S(1)} %get-tuple-element.5), channel_id=1, source_target_pairs={{0,2},{2,4},{4,6},{6,8},{8,10},{10,12},{12,14},{14,16},{16,18},{18... | collective-permute-start | bytes 6152 | tf_op jit(solution)/shard_map/ppermute | solution.py:21
  13.7 1.3 collective-permute-start.2
  15.1 0.7 convert_element_type.58
  15.9 0.8 fusion.24
  16.7 0.7 pad_maximum_fusion.2
  17.4 17.6 %all-gather = f32[512,8]{0,1:T(8,128)S(1)} all-gather(f32[128,8]{0,1:T(8,128)S(1)} %pad_maximum_fusion.2), channel_id=2, replica_groups={{0,8,16,24},{2,10,18,26},{4,12,20,28},{6,14,22,30},{1,9,17,25},{3,11,19..., dimensions={0}, use_global_device_ids=true | all-gather | bytes 20480 | tf_op jit(solution)/shard_map/all_gather | solution.py:237
  35.0 0.5 gather_fusion
  35.8 0.2 bitcast_select_fusion.1
  36.2 0.2 copy.27
  36.4 0.8 fusion.8.rest_0_
  37.3 0.8 select_convert_fusion.rest_1_
  38.0 1.3 pad_maximum_fusion.3
  39.5 0.3 fusion.4
  39.7 3.9 %all_to_all.19 = bf16[2,128,512]{2,1,0:T(8,128)(2,1)S(1)} all-to-all(bf16[2,128,512]{2,1,0:T(8,128)(2,1)S(1)} %bitcast.38), channel_id=1, replica_groups=mesh['sp'=16,'tp'=2] {'tp'}, dimensions={0} | all-to-all | bytes 524288 | tf_op jit(solution)/shard_map/all_to_all | solution.py:293
  43.7 0.2 copy.26
  43.9 3.0 %multiply_reduce_fusion = (f32[128]{0:T(128)S(1)}, f32[128,2048]{1,0:T(8,128)S(1)}) fusion(bf16[128,1024]{0,1:T(8,128)(2,1)S(1)} %bitcast.35, bf16[1024,2048]{1,0:T(8,128)(2,1)} %param.18, bf16[128,2048]{1,0:T(8,128)(2,1)S(1)} %copy-done.1), kind=kOutput, calls=%fused_computation.4 | convolution fusion | flops 537919360 | bytes 6029824 | tf_op jit(solution)/shard_map/dot_general | solution.py:294
  46.9 1.1 multiply_convert_fusion.normed
  48.0 132.5 %moe_exchange.1 = bf16[128,2048]{1,0:T(8,128)(2,1)} custom-call(bf16[128,2048]{1,0:T(8,128)(2,1)} %multiply_convert_fusion.normed, f32[128,2048]{1,0:T(8,128)} %copy-done, bf16[4,256,128]{2,1,0:T(8,128)(2,1)} %fusion.8.rest_0_, bf16[4,128,256]{2,1,0:T(8,128)(2,1)} %select_convert_fusion.rest_1_, bf16[2048,768]{1,0:T(8,128)(2,1)} %bitcast.31, ...), custom_call_target="tpu_custom_call" | custom-call | tf_op jit(solution)/shard_map/moe_exchange/pallas_call | solution.py:201
  180.5 1.9 %copy.30 = bf16[128,2048]{1,0:T(8,128)(2,1)} copy(bf16[128,2048]{1,0:T(8,128)(2,1)} %moe_exchange.1) | data formatting | bytes 1048576
  (30 shorter events, 0.6 us)
Async XLA Ops:
  0.0 39.4 %copy-start.4 = (s32[256]{0:T(256)S(1)}, s32[256]{0:T(256)}, u32[]{:S(2)}) copy-start(s32[256]{0:T(256)} %param.17) | copy-start | bytes 3076
  0.0 39.5 %copy-start.2 = (bf16[256,512]{1,0:T(8,128)(2,1)S(1)}, bf16[256,512]{1,0:T(8,128)(2,1)}, u32[]{:S(2)}) copy-start(bf16[256,512]{1,0:T(8,128)(2,1)} %param.14) | copy-start | bytes 786436
  0.0 43.9 %copy-start.1 = (bf16[128,2048]{1,0:T(8,128)(2,1)S(1)}, bf16[128,2048]{1,0:T(8,128)(2,1)}, u32[]{:S(2)}) copy-start(bf16[128,2048]{1,0:T(8,128)(2,1)} %param.19) | copy-start | bytes 1572868
  1.3 36.7 %collective-permute-start.1 = (f32[1]{0:T(128)}, f32[1]{0:T(128)}, u32[]{:S(2)}, u32[]{:S(2)}) collective-permute-start(f32[1]{0:T(128)} %get-tuple-element.16), channel_id=1, source_target_pairs={{0,2},{2,4},{4,6},{6,8},{8,10},{10,12},{12,14},{14,16},{16,18},{18... | collective-permute-start | bytes 20 | tf_op jit(solution)/shard_map/ppermute | solution.py:21
  6.8 31.3 %collective-permute-start.3 = (f32[1]{0:T(128)}, f32[1]{0:T(128)}, u32[]{:S(2)}, u32[]{:S(2)}) collective-permute-start(f32[1]{0:T(128)} %get-tuple-element.17), channel_id=1, source_target_pairs={{2,0},{4,2},{6,4},{8,6},{10,8},{12,10},{14,12},{16,14},{18,16},{20... | collective-permute-start | bytes 20 | tf_op jit(solution)/shard_map/ppermute | solution.py:22
  9.2 30.3 %collective-permute-start = (f32[1,512]{1,0:T(1,128)S(1)}, f32[1,512]{1,0:T(1,128)S(1)}, u32[]{:S(2)}, u32[]{:S(2)}) collective-permute-start(f32[1,512]{1,0:T(1,128)S(1)} %get-tuple-element.5), channel_id=1, source_target_pairs={{0,2},{2,4},{4,6},{6,8},{8,10},{10,12},{12,14},{14,16},{16,18},{18... | collective-permute-start | bytes 6152 | tf_op jit(solution)/shard_map/ppermute | solution.py:21
  13.7 25.7 %collective-permute-start.2 = (f32[1,512]{1,0:T(1,128)S(1)}, f32[1,512]{1,0:T(1,128)S(1)}, u32[]{:S(2)}, u32[]{:S(2)}) collective-permute-start(f32[1,512]{1,0:T(1,128)S(1)} %get-tuple-element.6), channel_id=1, source_target_pairs={{2,0},{4,2},{6,4},{8,6},{10,8},{12,10},{14,12},{16,14},{18,16},{20... | collective-permute-start | bytes 6152 | tf_op jit(solution)/shard_map/ppermute | solution.py:22
  38.0 8.9 %copy-start.3 = (f32[2048]{0:T(1024)S(1)}, f32[2048]{0:T(1024)}, u32[]{:S(2)}) copy-start(f32[2048]{0:T(1024)} %param.20) | copy-start | bytes 24580
  46.9 1.2 copy-start
where the time goes:
time: 183 us; the launch traced here: 182 us
  Pallas kernels  132 us (72%)
  blocking collectives  21.6 us (12%)
  starting transfers between devices  12.5 us (7%)
  other arithmetic  7.82 us (4%)
  local copies, waits for them, and re-layouts  4.54 us (2%)
  matrix products  3.21 us (2%)
    pallas_call x1, Pallas kernels, moe(): pl.pallas_call(body, out_shape=jax.ShapeDtypeStruct((block, width), bf),...  132 us
    all_gather x1, blocking collectives, slot_matrices(): every = lax.all_gather(packed, 'sp', axis_index_groups=groups)  17.6 us
    ppermute x2, starting transfers between devices, with_halo(): before = lax.ppermute(last, axis, up)  9.97 us
    all_to_all x1, blocking collectives, per_device(): lax.all_to_all(mixed, 'tp', split_axis=0, concat_axis=1, tiled=True)  3.94 us
  transfers between devices with their start and end apart: 4, of which 0 were waited for; matrix products, arithmetic and copies ran while one was open for 4% of the time, Pallas kernels for 0%

commit v1 on v0

v1 whole, which is shorter than its diff:
```python
import functools
import math

import jax
import jax.numpy as jnp
from jax import lax
from jax.experimental import pallas as pl
from jax.experimental.pallas import tpu as pltpu
from jax.sharding import PartitionSpec as P

MESH = pl.DeviceIdType.MESH
HALO = 16
BF = jnp.bfloat16
F32 = jnp.float32


def dot(a, b):
    return jnp.dot(a, b, preferred_element_type=F32)


def tile_of(size, most):
    return next(t for t in range(most, 0, -128) if size % t == 0)


def nearest_first(nz):
    return [sorted(range(nz), key=lambda b: (abs(b - z), abs(2 * b - nz + 1) * (1 if nz > 2 else 0), b))
            for z in range(nz)]


def layer_kernel(
    n_seq, nz, n_plane, n_core, cap, col,
    ci_hbm, go_hbm, gi_hbm, taps_hbm, docs_hbm, wp_hbm, stream_hbm, gain_hbm,
    routes_hbm, rw_hbm, wg_hbm, wu_hbm, wd_hbm,
    out_ref,
    wg, wu, wd, wp, ci_f, gi_f, go_f, taps_f, docs, prod, mixed, stream, gain, hidden,
    rbuf, wbuf, select, spread, zbuf, outgoing, arrived, act, returned, partial, summed,
    l_sem, e_send, e_recv, h_send, h_recv, d_send, d_recv, rt_send, rt_recv,
    zu_send, zd_send, z_recv, a_send, a_recv, r_send, r_recv, p_send, p_recv,
):
    peers = n_plane * n_core
    rows = peers * cap
    block, width = hidden.shape
    ff = wg.shape[1]
    half = ci_hbm.shape[1]
    span = block + HALO
    nc = width // col
    me = lax.axis_index("sp")
    core = lax.axis_index("tp")
    z, p = me // n_plane, lax.rem(me, n_plane)
    rank = p * n_core + core
    other = 1 - core

    def at_z(b):
        return {"sp": b * n_plane + p, "tp": core}

    def plane_peer(j):
        q = lax.rem(rank + j, peers)
        return {"sp": z * n_plane + q // n_core, "tp": lax.rem(q, n_core)}

    nxt, prv = lax.rem(me + 1, n_seq), lax.rem(me + n_seq - 1, n_seq)
    order = nearest_first(nz)

    def ordered(k):
        total = jnp.int32(0)
        for i in range(nz):
            total = total + jnp.where(z == i, order[i][k], 0)
        return total

    def remote(src, dst, send, recv, to):
        return pltpu.make_async_remote_copy(
            src_ref=src, dst_ref=dst, send_sem=send, recv_sem=recv,
            device_id=to, device_id_type=MESH)

    mine = pl.multiple_of(core * (block - HALO), HALO)
    theirs = pl.multiple_of(other * (block - HALO), HALO)
    my_at = pl.multiple_of(other * HALO, HALO)
    their_at = pl.multiple_of(core * HALO, HALO)

    def local(i, src, dst):
        return pltpu.make_async_copy(src, dst, l_sem.at[i])

    front = [
        local(0, ci_hbm.at[pl.ds(mine, span)], ci_f.at[core, pl.ds(my_at, span)]),
        local(1, gi_hbm.at[pl.ds(mine, span)], gi_f.at[core, pl.ds(my_at, span)]),
        local(2, go_hbm.at[pl.ds(pl.multiple_of(core * block, HALO), block)], go_f.at[core]),
        local(3, taps_hbm, taps_f.at[core]),
        local(4, docs_hbm, docs.at[0]),
        local(5, stream_hbm, stream),
        local(6, gain_hbm, gain),
    ]
    tables = [local(7, routes_hbm, rbuf.at[z]), local(8, rw_hbm, wbuf.at[z])]
    project = local(9, wp_hbm, wp)
    weights = [local(10, wg_hbm, wg), local(11, wu_hbm, wu), local(12, wd_hbm, wd)]
    for load in front + tables + [project]:
        load.start()

    barrier = pltpu.get_barrier_semaphore()

    def greet(to):
        pl.semaphore_signal(barrier, inc=1, device_id=to, device_id_type=MESH)

    for k in range(1, nz):
        greet(at_z(lax.rem(z + k, nz)))
    for j in range(1, peers):
        greet(plane_peer(j))
    for n in (nxt, prv):
        for c in range(n_core):
            greet({"sp": n, "tp": jnp.int32(c)})
    pl.semaphore_wait(barrier, nz - 1 + peers - 1 + 2 * n_core)

    edge = ci_hbm.shape[0] - HALO
    far = block + HALO
    partner = {"tp": other}
    swaps, halos = [], []
    for i, (src, dst) in enumerate(((ci_hbm, ci_f), (gi_hbm, gi_f))):
        halos.append(remote(src.at[pl.ds(edge, HALO)], dst.at[core, pl.ds(0, HALO)],
                            h_send.at[0, i], h_recv.at[core, i], {"sp": nxt, "tp": jnp.int32(0)}))
        halos.append(remote(src.at[pl.ds(0, HALO)], dst.at[core, pl.ds(far, HALO)],
                            h_send.at[1, i], h_recv.at[core, i], {"sp": prv, "tp": jnp.int32(1)}))
    notes = [
        remote(docs_hbm, docs.at[1], d_send.at[0], d_recv.at[0], {"sp": nxt, "tp": core}),
        remote(docs_hbm, docs.at[2], d_send.at[1], d_recv.at[1], {"sp": prv, "tp": core}),
    ]
    for i, (src, dst) in enumerate(((ci_hbm, ci_f), (gi_hbm, gi_f))):
        swaps.append(remote(src.at[pl.ds(theirs, span)], dst.at[core, pl.ds(their_at, span)],
                            e_send.at[i], e_recv.at[i], partner))
    swaps.append(remote(go_hbm.at[pl.ds(pl.multiple_of(other * block, HALO), block)], go_f.at[core],
                        e_send.at[2], e_recv.at[2], partner))
    swaps.append(remote(taps_hbm, taps_f.at[core], e_send.at[3], e_recv.at[3], partner))
    for copy in halos + notes + swaps:
        copy.start()
    lists = []
    for k in range(1, nz):
        to = at_z(lax.rem(z + k, nz))
        lists.append(remote(routes_hbm, rbuf.at[z], rt_send.at[k, 0], rt_recv.at[k, 0], to))
        lists.append(remote(rw_hbm, wbuf.at[z], rt_send.at[k, 1], rt_recv.at[k, 1], to))
    for copy in lists:
        copy.start()
    for load in weights:
        load.start()

    lane = lax.broadcasted_iota(jnp.int32, (block, block), 1)
    sub = lax.broadcasted_iota(jnp.int32, (block, block), 0)
    below = (sub < lane).astype(BF)

    def slots(k):
        b = ordered(k)
        chosen, weight = rbuf[b], wbuf[b]
        topk = chosen.shape[0]
        group = lax.broadcasted_iota(jnp.int32, (peers, block), 0)
        expert = z * peers + lax.rem(rank + group, peers)
        named = jnp.zeros((peers, block), F32)
        share = jnp.zeros((peers, block), F32)
        for i in range(topk):
            hit = jnp.broadcast_to(chosen[i:i + 1], (peers, block)) == expert
            named = jnp.where(hit, 1.0, named)
            share = jnp.where(hit, jnp.broadcast_to(weight[i:i + 1], (peers, block)), share)
        place = dot(named.astype(BF), below)
        place = jnp.where(named > 0.0, place, -1.0)
        seat = lax.broadcasted_iota(jnp.int32, (cap, block), 0).astype(F32)
        pieces = []
        for j in range(peers):
            here = jnp.broadcast_to(place[j:j + 1], (cap, block)) == seat
            select[k, j * cap:(j + 1) * cap, :] = jnp.where(here, 1.0, 0.0).astype(BF)
            pieces.append(jnp.where(here, jnp.broadcast_to(share[j:j + 1], (cap, block)), 0.0))
        spread[k] = jnp.concatenate(pieces, axis=0).T.astype(BF)

    for load in tables:
        load.wait()
    slots(0)

    for load in front:
        load.wait()
    for copy in notes + swaps:
        copy.wait_recv()
    for h in range(n_core):
        for i, dst in enumerate((ci_f, gi_f)):
            here = dst.at[h, pl.ds(pl.multiple_of(core * far, HALO), HALO)]
            remote(here, here, h_send.at[0, i], h_recv.at[h, i], partner).wait_recv()

    own, before_docs, after_docs = docs[0], docs[1], docs[2]
    first_half = core == 0
    wide = (8, block)

    def row(x):
        return jnp.broadcast_to(x.astype(F32), wide)

    cur = row(jnp.where(first_half, own[0:1], own[1:2]))
    left = row(jnp.where(first_half, before_docs[1:2], own[0:1]))
    right = row(jnp.where(first_half, own[1:2], after_docs[0:1]))
    lanes = lax.broadcasted_iota(jnp.int32, wide, 1)
    before = jnp.where(lanes == 0, pltpu.roll(left, 1, 1), pltpu.roll(cur, 1, 1))
    after = jnp.where(lanes == block - 1, pltpu.roll(right, block - 1, 1), pltpu.roll(cur, block - 1, 1))
    position = (me * n_core + core) * block + lanes
    has_before = (cur == before) & (position > 0)
    has_after = (cur == after) & (position < n_seq * n_core * block - 1)
    both = jnp.where(lax.broadcasted_iota(jnp.int32, wide, 0) == 0,
                     jnp.where(has_before, 1.0, 0.0), jnp.where(has_after, 1.0, 0.0))
    marks = jnp.concatenate([both] * (block // 8), axis=0).T
    keep_before, keep_after = marks[:, 0:1], marks[:, 1:2]

    for h in range(n_core):
        prod[...] = gi_f[h].astype(F32) * ci_f[h].astype(F32)
        conv = (
            taps_f[h, 0:1, :] * (prod[HALO - 1:HALO - 1 + block, :] * keep_before)
            + taps_f[h, 1:2, :] * prod[HALO:HALO + block, :]
            + taps_f[h, 2:3, :] * (prod[HALO + 1:HALO + 1 + block, :] * keep_after)
        )
        mixed[:, h * half:(h + 1) * half] = (go_f[h].astype(F32) * conv).astype(BF)

    project.wait()
    square = jnp.zeros((block, 128), F32)
    for q in range(nc):
        cols = slice(q * col, (q + 1) * col)
        value = stream[:, cols].astype(F32) + dot(mixed[...], wp[:, cols])
        hidden[:, cols] = value
        value = value * value
        for i in range(col // 128):
            square = square + value[:, i * 128:(i + 1) * 128]
    scale = lax.rsqrt(jnp.sum(square, axis=1, keepdims=True) / width + 1e-05)

    def chunk(q):
        return pl.ds(pl.multiple_of(q * col, col), col)

    def z_up(h, q):
        b = z - h
        piece = zbuf.at[b, :, chunk(q)]
        return remote(piece, piece, zu_send.at[h, q], z_recv.at[b, q], at_z(z + 1))

    def z_down(h, q):
        b = z + h
        piece = zbuf.at[b, :, chunk(q)]
        return remote(piece, piece, zd_send.at[h, q], z_recv.at[b, q], at_z(z - 1))

    for q in range(nc):
        cols = slice(q * col, (q + 1) * col)
        zbuf[z, :, cols] = (hidden[:, cols] * scale * gain[:, cols]).astype(BF)

    for q in range(nc):
        @pl.when(z < nz - 1)
        def _():
            z_up(0, q).start()

        @pl.when(z > 0)
        def _():
            z_down(0, q).start()

    def pump(h, q):
        @pl.when(z >= h)
        def _():
            piece = zbuf.at[z - h, :, chunk(q)]
            remote(piece, piece, zu_send.at[h, q], z_recv.at[z - h, q], at_z(z)).wait_recv()

            @pl.when(z < nz - 1)
            def _():
                z_up(h, q).start()

        @pl.when(z + h < nz)
        def _():
            piece = zbuf.at[z + h, :, chunk(q)]
            remote(piece, piece, zd_send.at[h, q], z_recv.at[z + h, q], at_z(z)).wait_recv()

            @pl.when(z > 0)
            def _():
                z_down(h, q).start()

    def a_copy(k, j, q):
        return remote(
            outgoing.at[k, pl.ds((j - 1) * cap, cap), chunk(q)], arrived.at[k, pl.ds(j * cap, cap), chunk(q)],
            a_send.at[k, q], a_recv.at[k, q], plane_peer(j))

    def a_all(k, q):
        return remote(outgoing.at[k, :, chunk(q)], arrived.at[k, pl.ds(cap, rows - cap), chunk(q)],
                      a_send.at[k, q], a_recv.at[k, q], plane_peer(1))

    def r_copy(k, j, q):
        return remote(
            arrived.at[k, pl.ds(j * cap, cap), chunk(q)], returned.at[k, pl.ds(j * cap, cap), chunk(q)],
            r_send.at[k, q], r_recv.at[k, q], plane_peer(peers - j))

    def r_all(k, q):
        return remote(
            arrived.at[k, pl.ds(cap, rows - cap), chunk(q)], returned.at[k, pl.ds(cap, rows - cap), chunk(q)],
            r_send.at[k, q], r_recv.at[k, q], plane_peer(1))

    def dispatch(k):
        b = ordered(k)

        @pl.loop(0, nc)
        def _(q):
            if k:
                pump(k, q)
            cols = chunk(q)
            picked = dot(select[k], zbuf[b, :, cols]).astype(BF)
            arrived[k, 0:cap, cols] = picked[:cap]
            outgoing[k, :, cols] = picked[cap:]
            for j in range(1, peers):
                a_copy(k, j, q).start()

    fcol = tile_of(ff, 256)

    def expert(k):
        if k == 0:
            for load in weights:
                load.wait()

        @pl.loop(0, nc)
        def _(q):
            a_all(k, q).wait_recv()

        @pl.loop(0, ff // fcol)
        def _(i):
            cols = pl.ds(pl.multiple_of(i * fcol, fcol), fcol)
            gate = jnp.minimum(dot(arrived[k], wg[:, cols]), 7.0)
            upper = jnp.clip(dot(arrived[k], wu[:, cols]), -7.0, 7.0)
            act[:, cols] = ((upper + 1.0) * gate * jax.nn.sigmoid(1.702 * gate)).astype(BF)

        @pl.loop(0, nc)
        def _(q):
            cols = chunk(q)
            res = dot(act[...], wd[:, cols]).astype(BF)
            returned[k, 0:cap, cols] = res[:cap]
            arrived[k, cap:, cols] = res[cap:]
            if k:
                give(k, q)

    def give(k, q):
        for j in range(1, peers):
            r_copy(k, j, q).start()

    def p_copy(k, q):
        b = ordered(k)
        return remote(
            partial.at[k - 1, :, chunk(q)], summed.at[lax.rem(z - b + nz, nz) - 1, :, chunk(q)],
            p_send.at[k, q], p_recv.at[q], at_z(b))

    def combine(k):
        @pl.loop(0, nc)
        def _(q):
            cols = chunk(q)
            r_all(k, q).wait_recv()
            total = dot(spread[k], returned[k, :, cols])
            if k == 0:
                hidden[:, cols] = hidden[:, cols] + total
            else:
                partial[k - 1, :, cols] = total.astype(BF)
                p_copy(k, q).start()

    dispatch(0)
    for copy in lists:
        copy.wait_recv()
    for k in range(1, nz):
        slots(k)
        dispatch(k)
        expert(k - 1)
        if k >= 3:
            combine(k - 2)
    expert(nz - 1)

    @pl.loop(0, nc)
    def _(q):
        give(0, q)

    for k in range(max(1, nz - 2), nz):
        combine(k)
    combine(0)

    for q in range(nc):
        piece = summed.at[:, :, chunk(q)]
        remote(piece, piece, p_send.at[0, q], p_recv.at[q], at_z(z)).wait_recv()
        cols = slice(q * col, (q + 1) * col)
        total = hidden[:, cols]
        for i in range(nz - 1):
            total = total + summed[i, :, cols].astype(F32)
        out_ref[:, cols] = total.astype(BF)

    for copy in halos + notes + swaps + lists:
        copy.wait_send()

    @pl.loop(0, nc)
    def _(q):
        for h in range(nz):
            @pl.when((z >= h) & (z < nz - 1))
            def _():
                z_up(h, q).wait_send()

            @pl.when((z + h < nz) & (z > 0))
            def _():
                z_down(h, q).wait_send()
        for k in range(nz):
            a_all(k, q).wait_send()
            r_all(k, q).wait_send()
            if k:
                p_copy(k, q).wait_send()


def layer(n_seq, nz, n_plane, n_core, cap, *args):
    tok, half = args[0].shape
    block, width = args[6].shape
    ff = args[10].shape[1]
    peers = n_plane * n_core
    rows = peers * cap
    topk = args[8].shape[0]
    channels = half * n_core
    frame = block + 2 * HALO
    col = tile_of(width, 512)
    nc = width // col
    hbm = pl.BlockSpec(memory_space=pl.ANY)
    vmem = pl.BlockSpec(memory_space=pltpu.VMEM)
    dma = pltpu.SemaphoreType.DMA
    return pl.pallas_call(
        functools.partial(layer_kernel, n_seq, nz, n_plane, n_core, cap, col),
        out_shape=jax.ShapeDtypeStruct((block, width), BF),
        in_specs=[hbm] * len(args),
        out_specs=vmem,
        scratch_shapes=[
            pltpu.VMEM((width, ff), BF),
            pltpu.VMEM((width, ff), BF),
            pltpu.VMEM((ff, width), BF),
            pltpu.VMEM((channels, width), BF),
            pltpu.VMEM((n_core, frame, half), BF),
            pltpu.VMEM((n_core, frame, half), BF),
            pltpu.VMEM((n_core, block, half), BF),
            pltpu.VMEM((n_core,) + args[3].shape, F32),
            pltpu.VMEM((3, n_core, block), jnp.int32),
            pltpu.VMEM((frame, half), F32),
            pltpu.VMEM((block, channels), BF),
            pltpu.VMEM((block, width), BF),
            pltpu.VMEM((1, width), F32),
            pltpu.VMEM((block, width), F32),
            pltpu.VMEM((nz, topk, block), jnp.int32),
            pltpu.VMEM((nz, topk, block), F32),
            pltpu.VMEM((nz, rows, block), BF),
            pltpu.VMEM((nz, block, rows), BF),
            pltpu.VMEM((nz, block, width), BF),
            pltpu.VMEM((nz, rows - cap, width), BF),
            pltpu.VMEM((nz, rows, width), BF),
            pltpu.VMEM((rows, ff), BF),
            pltpu.VMEM((nz, rows, width), BF),
            pltpu.VMEM((nz - 1, block, width), BF),
            pltpu.VMEM((nz - 1, block, width), BF),
            dma((13,)), dma((4,)), dma((4,)), dma((2, 2)), dma((n_core, 2)),
            dma((2,)), dma((2,)), dma((nz, 2)), dma((nz, 2)),
            dma((nz, nc)), dma((nz, nc)), dma((nz, nc)),
            dma((nz, nc)), dma((nz, nc)), dma((nz, nc)), dma((nz, nc)),
            dma((nz, nc)), dma((nc,)),
        ],
        compiler_params=pltpu.CompilerParams(
            collective_id=0, has_side_effects=True, vmem_limit_bytes=62 * 2**20),
        name="mixer_experts",
    )(*args)


def per_device(
    conv_in, gate_outer, gate_inner, tap_weights, doc_ids, w_proj, stream, norm_gain,
    routes, route_weights, w_gate, w_up, w_down,
):
    n_seq = lax.axis_size("sp")
    n_core = lax.axis_size("tp")
    tok_dev = conv_in.shape[0]
    topk = routes.shape[1]
    capacity = max(2, 2 * tok_dev * topk // (n_core * n_seq * n_core))
    capacity = -(-capacity // 16) * 16
    nz = max(d for d in range(1, math.isqrt(n_seq) + 1) if n_seq % d == 0)
    return layer(
        n_seq, nz, n_seq // nz, n_core, capacity,
        conv_in, gate_outer, gate_inner, tap_weights,
        doc_ids.reshape(n_core, tok_dev // n_core), w_proj, stream, norm_gain.reshape(1, -1),
        routes.T, route_weights.T, w_gate[0], w_up[0], w_down[0])


def solution(mesh):
    in_specs = (
        P("sp", "tp"),
        P("sp", "tp"),
        P("sp", "tp"),
        P(None, "tp"),
        P("sp"),
        P(),
        P(("sp", "tp"), None),
        P(),
        P(("sp", "tp"), None),
        P(("sp", "tp"), None),
        P(("sp", "tp"), None, None),
        P(("sp", "tp"), None, None),
        P(("sp", "tp"), None, None),
    )
    return jax.shard_map(
        per_device, mesh=mesh, in_specs=in_specs, out_specs=P(("sp", "tp"), None), check_vma=False
    )
```

time: 183 us -> 117 us (0.64)
  blocking collectives: 21.6 us -> 0 us
  Pallas kernels: 132 us -> 115 us
  starting transfers between devices: 12.5 us -> 0 us
  other arithmetic: 7.82 us -> 0 us
  matrix products: 3.21 us -> 0 us
  local copies, waits for them, and re-layouts: 4.54 us -> 1.88 us
    pallas_call x1, Pallas kernels: 132 us -> 115 us  [layer(): pl.pallas_call(functools.partial(layer_kernel, n_seq, nz, n_plane, n_core...]
    all_gather x1 -> x0, blocking collectives: 17.6 us -> none  [slot_matrices(): every = lax.all_gather(packed, 'sp', axis_index_groups=groups)]
    ppermute x4 -> x0, starting transfers between devices: 12.5 us -> none  [the longest x2 9.97 us: with_halo(): before = lax.ppermute(last, axis, up)]
    convert_element_type x7 -> x0, other arithmetic: 4.48 us -> none  [the longest x1 1.12 us: per_device(): normed = (hidden * scale * norm_gain).astype(jnp.bfloat16)]
    all_to_all x1 -> x0, blocking collectives: 3.94 us -> none  [per_device(): lax.all_to_all(mixed, 'tp', split_axis=0, concat_axis=1, tiled=True)]
    dot_general x2 -> x0, matrix products: 3.21 us -> none  [the longest x1 3.01 us: per_device(): projected = jnp.dot(regrouped, w_proj, preferred_element_type=jnp.float32)]
    concatenate x2 -> x0, other arithmetic: 2.02 us -> none  [the longest x1 1.33 us: with_halo(): shard = jnp.concatenate([before, shard, after], axis=dim)]
  transfers between devices with their start and end apart: 4 -> 0, of which waited for: 0 -> 0; matrix products, arithmetic and copies ran while one was open for 4% -> 0% of each run, Pallas kernels for 0% -> 0%
where the time goes in v1:
time: 117 us; the launch traced here: 116 us
  Pallas kernels  115 us (98%)
  local copies, waits for them, and re-layouts  1.88 us (2%)
    pallas_call x1, Pallas kernels, layer(): pl.pallas_call(functools.partial(layer_kernel, n_seq, nz, n_plane, n_core...  115 us

profile of v1, /device:TPU:0, one launch (start us, length us, event | category | flops | bytes accessed | tf_op | source)
XLA Modules:
  0.0 116.4 jit_solution(900144111392778654)
XLA Ops:
  0.0 114.5 %mixer_experts.1 = bf16[128,2048]{1,0:T(8,128)(2,1)} custom-call(bf16[256,512]{1,0:T(8,128)(2,1)} %ci_hbm.1, bf16[256,512]{1,0:T(8,128)(2,1)} %go_hbm.1, bf16[256,512]{1,0:T(8,128)(2,1)} %gi_hbm.1, f32[3,512]{1,0:T(4,128)} %taps_hbm.1, s32[2,128]{1,0:T(2,128)} %bitcast.13, bf16[1024,2048]{1,0:T(8,128)(2,1)} %wp_hbm.1, bf16[128,2048]{1,0:T(8,128)(2,1)} %stream_hbm.1, ...), custom_call_target="tpu_custom_call" | custom-call | tf_op jit(solution)/shard_map/mixer_experts/pallas_call | solution.py:411
  114.5 1.9 %copy.15 = bf16[128,2048]{1,0:T(8,128)(2,1)} copy(bf16[128,2048]{1,0:T(8,128)(2,1)} %mixer_experts.1) | data formatting | bytes 1048576

commit v2 on v1

--- a/solution.py
+++ b/solution.py
@@ -33,7 +33,7 @@
     routes_hbm, rw_hbm, wg_hbm, wu_hbm, wd_hbm,
     out_ref,
     wg, wu, wd, wp, ci_f, gi_f, go_f, taps_f, docs, prod, mixed, stream, gain, hidden,
-    rbuf, wbuf, select, spread, zbuf, outgoing, arrived, act, returned, partial, summed,
+    rbuf, wbuf, select, spread, zbuf, outgoing, arrived, act, returned, partial, chain,
     l_sem, e_send, e_recv, h_send, h_recv, d_send, d_recv, rt_send, rt_recv,
     zu_send, zd_send, z_recv, a_send, a_recv, r_send, r_recv, p_send, p_recv,
 ):
@@ -91,7 +91,7 @@
     tables = [local(7, routes_hbm, rbuf.at[z]), local(8, rw_hbm, wbuf.at[z])]
     project = local(9, wp_hbm, wp)
     weights = [local(10, wg_hbm, wg), local(11, wu_hbm, wu), local(12, wd_hbm, wd)]
-    for load in front + tables + [project]:
+    for load in front + tables + [project] + weights:
         load.start()
 
     barrier = pltpu.get_barrier_semaphore()
@@ -136,8 +136,6 @@
         lists.append(remote(rw_hbm, wbuf.at[z], rt_send.at[k, 1], rt_recv.at[k, 1], to))
     for copy in lists:
         copy.start()
-    for load in weights:
-        load.start()
 
     lane = lax.broadcasted_iota(jnp.int32, (block, block), 1)
     sub = lax.broadcasted_iota(jnp.int32, (block, block), 0)
@@ -321,20 +319,30 @@
             res = dot(act[...], wd[:, cols]).astype(BF)
             returned[k, 0:cap, cols] = res[:cap]
             arrived[k, cap:, cols] = res[cap:]
-            if k:
+            if k == nz - 1:
                 give(k, q)
 
     def give(k, q):
         for j in range(1, peers):
             r_copy(k, j, q).start()
 
+    def chained(b):
+        return ((b < z) & (z < nz - 1)) | ((b > z) & (z > 0))
+
     def p_copy(k, q):
         b = ordered(k)
-        return remote(
-            partial.at[k - 1, :, chunk(q)], summed.at[lax.rem(z - b + nz, nz) - 1, :, chunk(q)],
-            p_send.at[k, q], p_recv.at[q], at_z(b))
+        down = b < z
+        seat = jnp.where(down & (b == z - 1), nz, b)
+        return remote(partial.at[k - 1, :, chunk(q)], chain.at[seat, :, chunk(q)],
+                      p_send.at[k, q], p_recv.at[seat, q], at_z(jnp.where(down, z - 1, z + 1)))
+
+    def p_wait(seat, q):
+        piece = chain.at[seat, :, chunk(q)]
+        remote(piece, piece, p_send.at[0, q], p_recv.at[seat, q], at_z(z)).wait_recv()
 
     def combine(k):
+        b = ordered(k)
+
         @pl.loop(0, nc)
         def _(q):
             cols = chunk(q)
@@ -343,7 +351,15 @@
             if k == 0:
                 hidden[:, cols] = hidden[:, cols] + total
             else:
-                partial[k - 1, :, cols] = total.astype(BF)
+                @pl.when(chained(b))
+                def _():
+                    p_wait(b, q)
+                    partial[k - 1, :, cols] = (total + chain[b, :, cols].astype(F32)).astype(BF)
+
+                @pl.when(jnp.logical_not(chained(b)))
+                def _():
+                    partial[k - 1, :, cols] = total.astype(BF)
+
                 p_copy(k, q).start()
 
     dispatch(0)
@@ -352,27 +368,38 @@
     for k in range(1, nz):
         slots(k)
         dispatch(k)
-        expert(k - 1)
-        if k >= 3:
-            combine(k - 2)
+        if k < nz - 1:
+            expert(k - 1)
+
+    def give_all(k, low, high):
+        @pl.loop(low, high)
+        def _(q):
+            give(k, q)
+
+    give_all(0, 0, nc // 2)
+    expert(nz - 2)
     expert(nz - 1)
+    for k in range(nz - 2, 0, -1):
+        give_all(k, 0, nc)
+    give_all(0, nc // 2, nc)
+    for k in range(nz - 1, -1, -1):
+        combine(k)
 
     @pl.loop(0, nc)
     def _(q):
-        give(0, q)
-
-    for k in range(max(1, nz - 2), nz):
-        combine(k)
-    combine(0)
-
-    for q in range(nc):
-        piece = summed.at[:, :, chunk(q)]
-        remote(piece, piece, p_send.at[0, q], p_recv.at[q], at_z(z)).wait_recv()
-        cols = slice(q * col, (q + 1) * col)
-        total = hidden[:, cols]
-        for i in range(nz - 1):
-            total = total + summed[i, :, cols].astype(F32)
-        out_ref[:, cols] = total.astype(BF)
+        cols = chunk(q)
+
+        @pl.when(z > 0)
+        def _():
+            p_wait(z, q)
+            hidden[:, cols] = hidden[:, cols] + chain[z, :, cols].astype(F32)
+
+        @pl.when(z < nz - 1)
+        def _():
+            p_wait(nz, q)
+            hidden[:, cols] = hidden[:, cols] + chain[nz, :, cols].astype(F32)
+
+        out_ref[:, cols] = hidden[:, cols].astype(BF)
 
     for copy in halos + notes + swaps + lists:
         copy.wait_send()
@@ -438,12 +465,12 @@
             pltpu.VMEM((rows, ff), BF),
             pltpu.VMEM((nz, rows, width), BF),
             pltpu.VMEM((nz - 1, block, width), BF),
-            pltpu.VMEM((nz - 1, block, width), BF),
+            pltpu.VMEM((nz + 1, block, width), BF),
             dma((13,)), dma((4,)), dma((4,)), dma((2, 2)), dma((n_core, 2)),
             dma((2,)), dma((2,)), dma((nz, 2)), dma((nz, 2)),
             dma((nz, nc)), dma((nz, nc)), dma((nz, nc)),
             dma((nz, nc)), dma((nz, nc)), dma((nz, nc)), dma((nz, nc)),
-            dma((nz, nc)), dma((nc,)),
+            dma((nz, nc)), dma((nz + 1, nc)),
         ],
         compiler_params=pltpu.CompilerParams(
             collective_id=0, has_side_effects=True, vmem_limit_bytes=62 * 2**20),

time: 117 us -> 110 us (0.940)
  Pallas kernels: 115 us -> 108 us
    pallas_call x1, Pallas kernels: 115 us -> 108 us  [layer(): pl.pallas_call(functools.partial(layer_kernel, n_seq, nz, n_plane, n_core...]
where the time goes in v2:
time: 110 us
  Pallas kernels  108 us (98%)
  local copies, waits for them, and re-layouts  1.88 us (2%)
    pallas_call x1, Pallas kernels, layer(): pl.pallas_call(functools.partial(layer_kernel, n_seq, nz, n_plane, n_core...  108 us

profile of v2, /device:TPU:0, one launch (start us, length us, event | category | flops | bytes accessed | tf_op | source)
XLA Modules:
  0.0 109.8 jit_solution(6692910300909543360)
XLA Ops:
  0.0 107.9 %mixer_experts.1 = bf16[128,2048]{1,0:T(8,128)(2,1)} custom-call(bf16[256,512]{1,0:T(8,128)(2,1)} %ci_hbm.1, bf16[256,512]{1,0:T(8,128)(2,1)} %go_hbm.1, bf16[256,512]{1,0:T(8,128)(2,1)} %gi_hbm.1, f32[3,512]{1,0:T(4,128)} %taps_hbm.1, s32[2,128]{1,0:T(2,128)} %bitcast.13, bf16[1024,2048]{1,0:T(8,128)(2,1)} %wp_hbm.1, bf16[128,2048]{1,0:T(8,128)(2,1)} %stream_hbm.1, ...), custom_call_target="tpu_custom_call" | custom-call | tf_op jit(solution)/shard_map/mixer_experts/pallas_call | solution.py:438
  107.9 1.9 %copy.15 = bf16[128,2048]{1,0:T(8,128)(2,1)} copy(bf16[128,2048]{1,0:T(8,128)(2,1)} %mixer_experts.1) | data formatting | bytes 1048576

commit v3 on v2

--- a/solution.py
+++ b/solution.py
@@ -10,6 +10,8 @@
 
 MESH = pl.DeviceIdType.MESH
 HALO = 16
+SLAB = 256
+COL = 896
 BF = jnp.bfloat16
 F32 = jnp.float32
 
@@ -28,14 +30,16 @@
 
 
 def layer_kernel(
-    n_seq, nz, n_plane, n_core, cap, col,
+    n_seq, nz, n_plane, n_core, cap, col, slab,
     ci_hbm, go_hbm, gi_hbm, taps_hbm, docs_hbm, wp_hbm, stream_hbm, gain_hbm,
     routes_hbm, rw_hbm, wg_hbm, wu_hbm, wd_hbm,
     out_ref,
     wg, wu, wd, wp, ci_f, gi_f, go_f, taps_f, docs, prod, mixed, stream, gain, hidden,
     rbuf, wbuf, select, spread, zbuf, outgoing, arrived, act, returned, partial, chain,
+    rbuf2, wbuf2, select2, spread2, pslab, outgoing2, returned2, partial2, summed2,
     l_sem, e_send, e_recv, h_send, h_recv, d_send, d_recv, rt_send, rt_recv,
     zu_send, zd_send, z_recv, a_send, a_recv, r_send, r_recv, p_send, p_recv,
+    rt2_send, rt2_recv, s_send, s_recv, v_send, v_recv, w_send, w_recv, f_send, f_recv,
 ):
     peers = n_plane * n_core
     rows = peers * cap
@@ -43,7 +47,9 @@
     ff = wg.shape[1]
     half = ci_hbm.shape[1]
     span = block + HALO
-    nc = width // col
+    main = width - slab
+    nc = main // col
+    wide_col = tile_of(width, 512)
     me = lax.axis_index("sp")
     core = lax.axis_index("tp")
     z, p = me // n_plane, lax.rem(me, n_plane)
@@ -52,6 +58,9 @@
 
     def at_z(b):
         return {"sp": b * n_plane + p, "tp": core}
+
+    def in_plane(q):
+        return {"sp": z * n_plane + q, "tp": core}
 
     def plane_peer(j):
         q = lax.rem(rank + j, peers)
@@ -88,7 +97,8 @@
         local(5, stream_hbm, stream),
         local(6, gain_hbm, gain),
     ]
-    tables = [local(7, routes_hbm, rbuf.at[z]), local(8, rw_hbm, wbuf.at[z])]
+    tables = [local(7, routes_hbm, rbuf.at[z]), local(8, rw_hbm, wbuf.at[z]),
+              local(13, routes_hbm, rbuf2.at[p]), local(14, rw_hbm, wbuf2.at[p])]
     project = local(9, wp_hbm, wp)
     weights = [local(10, wg_hbm, wg), local(11, wu_hbm, wu), local(12, wd_hbm, wd)]
     for load in front + tables + [project] + weights:
@@ -101,12 +111,13 @@
 
     for k in range(1, nz):
         greet(at_z(lax.rem(z + k, nz)))
+        greet({"sp": lax.rem(z + k, nz) * n_plane + p, "tp": other})
     for j in range(1, peers):
         greet(plane_peer(j))
     for n in (nxt, prv):
         for c in range(n_core):
             greet({"sp": n, "tp": jnp.int32(c)})
-    pl.semaphore_wait(barrier, nz - 1 + peers - 1 + 2 * n_core)
+    pl.semaphore_wait(barrier, 2 * (nz - 1) + peers - 1 + 2 * n_core)
 
     edge = ci_hbm.shape[0] - HALO
     far = block + HALO
@@ -134,6 +145,10 @@
         to = at_z(lax.rem(z + k, nz))
         lists.append(remote(routes_hbm, rbuf.at[z], rt_send.at[k, 0], rt_recv.at[k, 0], to))
         lists.append(remote(rw_hbm, wbuf.at[z], rt_send.at[k, 1], rt_recv.at[k, 1], to))
+    for i in range(1, n_plane):
+        to = in_plane(lax.rem(p + i, n_plane))
+        lists.append(remote(routes_hbm, rbuf2.at[p], rt2_send.at[i, 0], rt2_recv.at[i, 0], to))
+        lists.append(remote(rw_hbm, wbuf2.at[p], rt2_send.at[i, 1], rt2_recv.at[i, 1], to))
     for copy in lists:
         copy.start()
 
@@ -141,31 +156,46 @@
     sub = lax.broadcasted_iota(jnp.int32, (block, block), 0)
     below = (sub < lane).astype(BF)
 
-    def slots(k):
-        b = ordered(k)
-        chosen, weight = rbuf[b], wbuf[b]
-        topk = chosen.shape[0]
-        group = lax.broadcasted_iota(jnp.int32, (peers, block), 0)
-        expert = z * peers + lax.rem(rank + group, peers)
-        named = jnp.zeros((peers, block), F32)
-        share = jnp.zeros((peers, block), F32)
-        for i in range(topk):
-            hit = jnp.broadcast_to(chosen[i:i + 1], (peers, block)) == expert
+    def slots(chosen, weight, expert, put):
+        count = expert.shape[0]
+        named = jnp.zeros((count, block), F32)
+        share = jnp.zeros((count, block), F32)
+        for i in range(chosen.shape[0]):
+            hit = jnp.broadcast_to(chosen[i:i + 1], (count, block)) == expert
             named = jnp.where(hit, 1.0, named)
-            share = jnp.where(hit, jnp.broadcast_to(weight[i:i + 1], (peers, block)), share)
+            share = jnp.where(hit, jnp.broadcast_to(weight[i:i + 1], (count, block)), share)
         place = dot(named.astype(BF), below)
         place = jnp.where(named > 0.0, place, -1.0)
         seat = lax.broadcasted_iota(jnp.int32, (cap, block), 0).astype(F32)
-        pieces = []
-        for j in range(peers):
+        chosen_rows, pieces = [], []
+        for j in range(count):
             here = jnp.broadcast_to(place[j:j + 1], (cap, block)) == seat
-            select[k, j * cap:(j + 1) * cap, :] = jnp.where(here, 1.0, 0.0).astype(BF)
+            chosen_rows.append(jnp.where(here, 1.0, 0.0).astype(BF))
             pieces.append(jnp.where(here, jnp.broadcast_to(share[j:j + 1], (cap, block)), 0.0))
-        spread[k] = jnp.concatenate(pieces, axis=0).T.astype(BF)
+        put(jnp.concatenate(chosen_rows, axis=0), jnp.concatenate(pieces, axis=0).T.astype(BF))
+
+    def line_slots(k):
+        b = ordered(k)
+        group = lax.broadcasted_iota(jnp.int32, (peers, block), 0)
+
+        def put(pick, share):
+            select[k] = pick
+            spread[k] = share
+
+        slots(rbuf[b], wbuf[b], z * peers + lax.rem(rank + group, peers), put)
+
+    def plane_slots(q):
+        group = lax.broadcasted_iota(jnp.int32, (nz * n_core, block), 0)
+
+        def put(pick, share):
+            select2[q] = pick
+            spread2[q] = share
+
+        slots(rbuf2[q], wbuf2[q], group // n_core * peers + p * n_core + lax.rem(group, n_core), put)
 
     for load in tables:
         load.wait()
-    slots(0)
+    line_slots(0)
 
     for load in front:
         load.wait()
@@ -208,12 +238,12 @@
 
     project.wait()
     square = jnp.zeros((block, 128), F32)
-    for q in range(nc):
-        cols = slice(q * col, (q + 1) * col)
+    for q in range(width // wide_col):
+        cols = slice(q * wide_col, (q + 1) * wide_col)
         value = stream[:, cols].astype(F32) + dot(mixed[...], wp[:, cols])
         hidden[:, cols] = value
         value = value * value
-        for i in range(col // 128):
+        for i in range(wide_col // 128):
             square = square + value[:, i * 128:(i + 1) * 128]
     scale = lax.rsqrt(jnp.sum(square, axis=1, keepdims=True) / width + 1e-05)
 
@@ -230,9 +260,20 @@
         piece = zbuf.at[b, :, chunk(q)]
         return remote(piece, piece, zd_send.at[h, q], z_recv.at[b, q], at_z(z - 1))
 
+    def normed(cols):
+        return (hidden[:, cols] * scale * gain[:, cols]).astype(BF)
+
+    side = slice(main, width)
+    pslab[p] = normed(side)
+    s_copies = [
+        remote(pslab.at[p], pslab.at[p], s_send.at[i], s_recv.at[p], in_plane(lax.rem(p + i, n_plane)))
+        for i in range(1, n_plane)
+    ]
+    for copy in s_copies:
+        copy.start()
     for q in range(nc):
         cols = slice(q * col, (q + 1) * col)
-        zbuf[z, :, cols] = (hidden[:, cols] * scale * gain[:, cols]).astype(BF)
+        zbuf[z, :, cols] = normed(cols)
 
     for q in range(nc):
         @pl.when(z < nz - 1)
@@ -262,24 +303,34 @@
             def _():
                 z_down(h, q).start()
 
+    def seat_of(source):
+        return pl.multiple_of((lax.rem(source, n_core) * n_plane + source // n_core) * cap, HALO)
+
+    my_seat = seat_of(rank)
+
     def a_copy(k, j, q):
+        b = ordered(k)
         return remote(
-            outgoing.at[k, pl.ds((j - 1) * cap, cap), chunk(q)], arrived.at[k, pl.ds(j * cap, cap), chunk(q)],
-            a_send.at[k, q], a_recv.at[k, q], plane_peer(j))
+            outgoing.at[k, pl.ds((j - 1) * cap, cap), chunk(q)], arrived.at[b, pl.ds(my_seat, cap), chunk(q)],
+            a_send.at[b, q], a_recv.at[b, q], plane_peer(j))
 
     def a_all(k, q):
-        return remote(outgoing.at[k, :, chunk(q)], arrived.at[k, pl.ds(cap, rows - cap), chunk(q)],
-                      a_send.at[k, q], a_recv.at[k, q], plane_peer(1))
+        b = ordered(k)
+        return remote(outgoing.at[k, :, chunk(q)], arrived.at[b, pl.ds(cap, rows - cap), chunk(q)],
+                      a_send.at[b, q], a_recv.at[b, q], plane_peer(1))
 
     def r_copy(k, j, q):
+        b = ordered(k)
+        seat = seat_of(lax.rem(rank + peers - j, peers))
         return remote(
-            arrived.at[k, pl.ds(j * cap, cap), chunk(q)], returned.at[k, pl.ds(j * cap, cap), chunk(q)],
-            r_send.at[k, q], r_recv.at[k, q], plane_peer(peers - j))
+            arrived.at[b, pl.ds(seat, cap), chunk(q)], returned.at[b, pl.ds(j * cap, cap), chunk(q)],
+            r_send.at[b, q], r_recv.at[b, q], plane_peer(peers - j))
 
     def r_all(k, q):
+        b = ordered(k)
         return remote(
-            arrived.at[k, pl.ds(cap, rows - cap), chunk(q)], returned.at[k, pl.ds(cap, rows - cap), chunk(q)],
-            r_send.at[k, q], r_recv.at[k, q], plane_peer(1))
+            arrived.at[b, pl.ds(cap, rows - cap), chunk(q)], returned.at[b, pl.ds(cap, rows - cap), chunk(q)],
+            r_send.at[b, q], r_recv.at[b, q], plane_peer(1))
 
     def dispatch(k):
         b = ordered(k)
@@ -290,17 +341,91 @@
                 pump(k, q)
             cols = chunk(q)
             picked = dot(select[k], zbuf[b, :, cols]).astype(BF)
-            arrived[k, 0:cap, cols] = picked[:cap]
+            arrived[b, pl.ds(my_seat, cap), cols] = picked[:cap]
             outgoing[k, :, cols] = picked[cap:]
             for j in range(1, peers):
                 a_copy(k, j, q).start()
 
+    lot = n_plane * cap
+    side_ref = pl.ds(main, slab)
+    my_lot = pl.multiple_of(core * lot, HALO)
+    other_lot = pl.multiple_of(other * lot, HALO)
+
+    def v_copy(b, c):
+        return remote(
+            outgoing2.at[b, c], arrived.at[z, pl.ds(my_lot, lot), side_ref],
+            v_send.at[b, c], v_recv.at[z, core], {"sp": b * n_plane + p, "tp": c})
+
+    def v_wait(b, c):
+        piece = arrived.at[b, pl.ds(pl.multiple_of(c * lot, HALO), lot), side_ref]
+        remote(piece, piece, v_send.at[b, c], v_recv.at[b, c], partner).wait_recv()
+
+    def side_pick():
+        for q in range(n_plane):
+            @pl.when(p != q)
+            def _():
+                remote(pslab.at[q], pslab.at[q], s_send.at[1], s_recv.at[q], partner).wait_recv()
+
+            plane_slots(q)
+            picked = dot(select2[q], pslab[q]).astype(BF)
+            for b in range(nz):
+                for c in range(n_core):
+                    at = (b * n_core + c) * cap
+                    outgoing2[b, c, q * cap:(q + 1) * cap, :] = picked[at:at + cap]
+        arrived[z, pl.ds(my_lot, lot), side] = outgoing2[z, core]
+        v_copy(z, other).start()
+
+    def side_send(h):
+        @pl.when(z + h < nz)
+        def _():
+            for c in range(n_core):
+                v_copy(z + h, jnp.int32(c)).start()
+
+        @pl.when(z >= h)
+        def _():
+            for c in range(n_core):
+                v_copy(z - h, jnp.int32(c)).start()
+
+    def w_copy(b, c):
+        piece = arrived.at[b, pl.ds(pl.multiple_of(c * lot, HALO), lot), side_ref]
+        return remote(piece, returned2.at[z, core], w_send.at[b, c], w_recv.at[z, core],
+                      {"sp": b * n_plane + p, "tp": c})
+
+    def f_copy(q):
+        return remote(partial2.at[q], summed2.at[p], f_send.at[q], f_recv.at[p], in_plane(q))
+
+    def side_combine():
+        for b in range(nz):
+            for c in range(n_core):
+                @pl.when((z != b) | (core != c))
+                def _():
+                    piece = returned2.at[b, c]
+                    remote(piece, piece, w_send.at[b, c], w_recv.at[b, c], partner).wait_recv()
+        for q in range(n_plane):
+            results = jnp.concatenate(
+                [returned2[b, c, q * cap:(q + 1) * cap, :] for b in range(nz) for c in range(n_core)], axis=0)
+            total = dot(spread2[q], results)
+
+            @pl.when(p == q)
+            def _():
+                hidden[:, side] = hidden[:, side] + total
+
+            @pl.when(p != q)
+            def _():
+                partial2[q] = total.astype(BF)
+                f_copy(jnp.int32(q)).start()
+
     fcol = tile_of(ff, 256)
 
     def expert(k):
+        b = ordered(k)
         if k == 0:
             for load in weights:
                 load.wait()
+            v_wait(z, other)
+        else:
+            for c in range(n_core):
+                v_wait(b, c)
 
         @pl.loop(0, nc)
         def _(q):
@@ -309,16 +434,23 @@
         @pl.loop(0, ff // fcol)
         def _(i):
             cols = pl.ds(pl.multiple_of(i * fcol, fcol), fcol)
-            gate = jnp.minimum(dot(arrived[k], wg[:, cols]), 7.0)
-            upper = jnp.clip(dot(arrived[k], wu[:, cols]), -7.0, 7.0)
+            gate = jnp.minimum(dot(arrived[b], wg[:, cols]), 7.0)
+            upper = jnp.clip(dot(arrived[b], wu[:, cols]), -7.0, 7.0)
             act[:, cols] = ((upper + 1.0) * gate * jax.nn.sigmoid(1.702 * gate)).astype(BF)
+
+        arrived[b, :, side] = dot(act[...], wd[:, side]).astype(BF)
+        if k == 0:
+            returned2[z, core] = arrived[z, pl.ds(my_lot, lot), side]
+            w_copy(z, other).start()
+        else:
+            for c in range(n_core):
+                w_copy(b, c).start()
 
         @pl.loop(0, nc)
         def _(q):
             cols = chunk(q)
-            res = dot(act[...], wd[:, cols]).astype(BF)
-            returned[k, 0:cap, cols] = res[:cap]
-            arrived[k, cap:, cols] = res[cap:]
+            arrived[b, :, cols] = dot(act[...], wd[:, cols]).astype(BF)
+            returned[b, 0:cap, cols] = arrived[b, pl.ds(my_seat, cap), cols]
             if k == nz - 1:
                 give(k, q)
 
@@ -347,7 +479,7 @@
         def _(q):
             cols = chunk(q)
             r_all(k, q).wait_recv()
-            total = dot(spread[k], returned[k, :, cols])
+            total = dot(spread[k], returned[b, :, cols])
             if k == 0:
                 hidden[:, cols] = hidden[:, cols] + total
             else:
@@ -365,9 +497,11 @@
     dispatch(0)
     for copy in lists:
         copy.wait_recv()
+    side_pick()
     for k in range(1, nz):
-        slots(k)
+        line_slots(k)
         dispatch(k)
+        side_send(k)
         if k < nz - 1:
             expert(k - 1)
 
@@ -381,9 +515,17 @@
     expert(nz - 1)
     for k in range(nz - 2, 0, -1):
         give_all(k, 0, nc)
+    combine(nz - 1)
+    side_combine()
     give_all(0, nc // 2, nc)
-    for k in range(nz - 1, -1, -1):
+    for k in range(nz - 2, -1, -1):
         combine(k)
+    for q in range(n_plane):
+        @pl.when(p != q)
+        def _():
+            remote(summed2.at[q], summed2.at[q], f_send.at[q], f_recv.at[q], partner).wait_recv()
+            hidden[:, side] = hidden[:, side] + summed2[q].astype(F32)
+    out_ref[:, side] = hidden[:, side].astype(BF)
 
     @pl.loop(0, nc)
     def _(q):
@@ -401,8 +543,18 @@
 
         out_ref[:, cols] = hidden[:, cols].astype(BF)
 
-    for copy in halos + notes + swaps + lists:
+    for copy in halos + notes + swaps + lists + s_copies:
         copy.wait_send()
+    for b in range(nz):
+        for c in range(n_core):
+            @pl.when((z != b) | (core != c))
+            def _():
+                v_copy(jnp.int32(b), jnp.int32(c)).wait_send()
+                w_copy(jnp.int32(b), jnp.int32(c)).wait_send()
+    for q in range(n_plane):
+        @pl.when(p != q)
+        def _():
+            f_copy(jnp.int32(q)).wait_send()
 
     @pl.loop(0, nc)
     def _(q):
@@ -430,13 +582,16 @@
     topk = args[8].shape[0]
     channels = half * n_core
     frame = block + 2 * HALO
-    col = tile_of(width, 512)
-    nc = width // col
+    slab = SLAB if width > 2 * SLAB else 128
+    main = width - slab
+    col = tile_of(main, COL)
+    nc = main // col
+    lot = n_plane * cap
     hbm = pl.BlockSpec(memory_space=pl.ANY)
     vmem = pl.BlockSpec(memory_space=pltpu.VMEM)
     dma = pltpu.SemaphoreType.DMA
     return pl.pallas_call(
-        functools.partial(layer_kernel, n_seq, nz, n_plane, n_core, cap, col),
+        functools.partial(layer_kernel, n_seq, nz, n_plane, n_core, cap, col, slab),
         out_shape=jax.ShapeDtypeStruct((block, width), BF),
         in_specs=[hbm] * len(args),
         out_specs=vmem,
@@ -459,18 +614,30 @@
             pltpu.VMEM((nz, topk, block), F32),
             pltpu.VMEM((nz, rows, block), BF),
             pltpu.VMEM((nz, block, rows), BF),
-            pltpu.VMEM((nz, block, width), BF),
-            pltpu.VMEM((nz, rows - cap, width), BF),
+            pltpu.VMEM((nz, block, main), BF),
+            pltpu.VMEM((nz, rows - cap, main), BF),
             pltpu.VMEM((nz, rows, width), BF),
             pltpu.VMEM((rows, ff), BF),
-            pltpu.VMEM((nz, rows, width), BF),
-            pltpu.VMEM((nz - 1, block, width), BF),
-            pltpu.VMEM((nz + 1, block, width), BF),
-            dma((13,)), dma((4,)), dma((4,)), dma((2, 2)), dma((n_core, 2)),
+            pltpu.VMEM((nz, rows, main), BF),
+            pltpu.VMEM((nz - 1, block, main), BF),
+            pltpu.VMEM((nz + 1, block, main), BF),
+            pltpu.VMEM((n_plane, topk, block), jnp.int32),
+            pltpu.VMEM((n_plane, topk, block), F32),
+            pltpu.VMEM((n_plane, nz * n_core * cap, block), BF),
+            pltpu.VMEM((n_plane, block, nz * n_core * cap), BF),
+            pltpu.VMEM((n_plane, block, slab), BF),
+            pltpu.VMEM((nz, n_core, lot, slab), BF),
+            pltpu.VMEM((nz, n_core, lot, slab), BF),
+            pltpu.VMEM((n_plane, block, slab), BF),
+            pltpu.VMEM((n_plane, block, slab), BF),
+            dma((15,)), dma((4,)), dma((4,)), dma((2, 2)), dma((n_core, 2)),
             dma((2,)), dma((2,)), dma((nz, 2)), dma((nz, 2)),
             dma((nz, nc)), dma((nz, nc)), dma((nz, nc)),
             dma((nz, nc)), dma((nz, nc)), dma((nz, nc)), dma((nz, nc)),
             dma((nz, nc)), dma((nz + 1, nc)),
+            dma((n_plane, 2)), dma((n_plane, 2)), dma((n_plane,)), dma((n_plane,)),
+            dma((nz, n_core)), dma((nz, n_core)), dma((nz, n_core)), dma((nz, n_core)),
+            dma((n_plane,)), dma((n_plane,)),
         ],
         compiler_params=pltpu.CompilerParams(
             collective_id=0, has_side_effects=True, vmem_limit_bytes=62 * 2**20),

time: 110 us -> 104 us (0.945)
  Pallas kernels: 108 us -> 102 us
    pallas_call x1, Pallas kernels: 108 us -> 102 us  [layer(): pl.pallas_call(functools.partial(layer_kernel, n_seq, nz, n_plane, n_core...]
where the time goes in v3:
time: 104 us
  Pallas kernels  102 us (98%)
  local copies, waits for them, and re-layouts  1.88 us (2%)
    pallas_call x1, Pallas kernels, layer(): pl.pallas_call(functools.partial(layer_kernel, n_seq, nz, n_plane, n_core...  102 us

profile of v3, /device:TPU:0, one launch (start us, length us, event | category | flops | bytes accessed | tf_op | source)
XLA Modules:
  0.0 103.6 jit_solution(1333497937117720289)
XLA Ops:
  0.0 101.7 %mixer_experts.1 = bf16[128,2048]{1,0:T(8,128)(2,1)} custom-call(bf16[256,512]{1,0:T(8,128)(2,1)} %ci_hbm.1, bf16[256,512]{1,0:T(8,128)(2,1)} %go_hbm.1, bf16[256,512]{1,0:T(8,128)(2,1)} %gi_hbm.1, f32[3,512]{1,0:T(4,128)} %taps_hbm.1, s32[2,128]{1,0:T(2,128)} %bitcast.13, bf16[1024,2048]{1,0:T(8,128)(2,1)} %wp_hbm.1, bf16[128,2048]{1,0:T(8,128)(2,1)} %stream_hbm.1, ...), custom_call_target="tpu_custom_call" | custom-call | tf_op jit(solution)/shard_map/mixer_experts/pallas_call | solution.py:593
  101.7 1.9 %copy.15 = bf16[128,2048]{1,0:T(8,128)(2,1)} copy(bf16[128,2048]{1,0:T(8,128)(2,1)} %mixer_experts.1) | data formatting | bytes 1048576

commit v4 on v3

--- a/solution.py
+++ b/solution.py
@@ -10,8 +10,8 @@
 
 MESH = pl.DeviceIdType.MESH
 HALO = 16
-SLAB = 256
-COL = 896
+SLAB = 384
+CHUNKS = 2
 BF = jnp.bfloat16
 F32 = jnp.float32
 
@@ -30,16 +30,16 @@
 
 
 def layer_kernel(
-    n_seq, nz, n_plane, n_core, cap, col, slab,
+    n_seq, nz, n_plane, n_core, cap, cuts, slab,
     ci_hbm, go_hbm, gi_hbm, taps_hbm, docs_hbm, wp_hbm, stream_hbm, gain_hbm,
     routes_hbm, rw_hbm, wg_hbm, wu_hbm, wd_hbm,
     out_ref,
-    wg, wu, wd, wp, ci_f, gi_f, go_f, taps_f, docs, prod, mixed, stream, gain, hidden,
+    wg, wu, wd, wp, raw, frames, go_f, taps_f, docs, prod, mixed, stream, gain, hidden,
     rbuf, wbuf, select, spread, zbuf, outgoing, arrived, act, returned, partial, chain,
     rbuf2, wbuf2, select2, spread2, pslab, outgoing2, returned2, partial2, summed2,
     l_sem, e_send, e_recv, h_send, h_recv, d_send, d_recv, rt_send, rt_recv,
-    zu_send, zd_send, z_recv, a_send, a_recv, r_send, r_recv, p_send, p_recv,
-    rt2_send, rt2_recv, s_send, s_recv, v_send, v_recv, w_send, w_recv, f_send, f_recv,
+    z_send, z_recv, a_send, a_recv, r_send, r_recv, p_send, p_recv,
+    s_send, s_recv, v_send, v_recv, w_send, w_recv, f_send, f_recv,
 ):
     peers = n_plane * n_core
     rows = peers * cap
@@ -48,7 +48,7 @@
     half = ci_hbm.shape[1]
     span = block + HALO
     main = width - slab
-    nc = main // col
+    nc = len(cuts)
     wide_col = tile_of(width, 512)
     me = lax.axis_index("sp")
     core = lax.axis_index("tp")
@@ -66,7 +66,7 @@
         q = lax.rem(rank + j, peers)
         return {"sp": z * n_plane + q // n_core, "tp": lax.rem(q, n_core)}
 
-    nxt, prv = lax.rem(me + 1, n_seq), lax.rem(me + n_seq - 1, n_seq)
+    nxt, prv = me + 1, me - 1
     order = nearest_first(nz)
 
     def ordered(k):
@@ -88,20 +88,31 @@
     def local(i, src, dst):
         return pltpu.make_async_copy(src, dst, l_sem.at[i])
 
+    hbm_in = (ci_hbm, gi_hbm)
     front = [
-        local(0, ci_hbm.at[pl.ds(mine, span)], ci_f.at[core, pl.ds(my_at, span)]),
-        local(1, gi_hbm.at[pl.ds(mine, span)], gi_f.at[core, pl.ds(my_at, span)]),
-        local(2, go_hbm.at[pl.ds(pl.multiple_of(core * block, HALO), block)], go_f.at[core]),
-        local(3, taps_hbm, taps_f.at[core]),
-        local(4, docs_hbm, docs.at[0]),
-        local(5, stream_hbm, stream),
-        local(6, gain_hbm, gain),
+        local(0, src.at[pl.ds(mine, span)], frames.at[i, core, pl.ds(my_at, span)]) for i, src in enumerate(hbm_in)
+    ] + [
+        local(1, go_hbm.at[pl.ds(pl.multiple_of(core * block, HALO), block)], go_f.at[core]),
+        local(2, taps_hbm, taps_f.at[core]),
+        local(3, stream_hbm, stream),
+        local(4, gain_hbm, gain),
     ]
-    tables = [local(7, routes_hbm, rbuf.at[z]), local(8, rw_hbm, wbuf.at[z]),
-              local(13, routes_hbm, rbuf2.at[p]), local(14, rw_hbm, wbuf2.at[p])]
-    project = local(9, wp_hbm, wp)
-    weights = [local(10, wg_hbm, wg), local(11, wu_hbm, wu), local(12, wd_hbm, wd)]
-    for load in front + tables + [project] + weights:
+    own_frames = frames.at[:, core, pl.ds(my_at, span)]
+    front_waits = [pltpu.make_async_copy(own_frames, own_frames, l_sem.at[0])] + front[2:]
+    papers = local(5, docs_hbm, docs.at[0])
+    stage = [local(6, src, raw.at[i]) for i, src in enumerate((ci_hbm, gi_hbm, go_hbm))]
+    stage_wait = pltpu.make_async_copy(raw, raw, l_sem.at[6])
+    tables = [local(7, routes_hbm, rbuf.at[z]), local(7, rw_hbm, wbuf.at[z]),
+              local(7, routes_hbm, rbuf2.at[p]), local(7, rw_hbm, wbuf2.at[p])]
+    topk = routes_hbm.shape[0]
+
+    def lists_of(count):
+        return hidden.at[pl.ds(0, 2 * topk), pl.ds(0, count * block)]
+
+    tables_wait = pltpu.make_async_copy(lists_of(2), lists_of(2), l_sem.at[7])
+    project = local(8, wp_hbm, wp)
+    weights = [local(9, wg_hbm, wg), local(10, wu_hbm, wu), local(11, wd_hbm, wd)]
+    for load in stage + [papers] + front + tables:
         load.start()
 
     barrier = pltpu.get_barrier_semaphore()
@@ -114,43 +125,73 @@
         greet({"sp": lax.rem(z + k, nz) * n_plane + p, "tp": other})
     for j in range(1, peers):
         greet(plane_peer(j))
-    for n in (nxt, prv):
-        for c in range(n_core):
-            greet({"sp": n, "tp": jnp.int32(c)})
-    pl.semaphore_wait(barrier, 2 * (nz - 1) + peers - 1 + 2 * n_core)
+    has_prv, has_nxt = me > 0, me < n_seq - 1
+    for n, there in ((nxt, has_nxt), (prv, has_prv)):
+        @pl.when(there)
+        def _():
+            for c in range(n_core):
+                greet({"sp": n, "tp": jnp.int32(c)})
+    sides = jnp.where(has_prv, n_core, 0) + jnp.where(has_nxt, n_core, 0)
+    pl.semaphore_wait(barrier, 2 * (nz - 1) + peers - 1 + sides)
 
     edge = ci_hbm.shape[0] - HALO
     far = block + HALO
     partner = {"tp": other}
-    swaps, halos = [], []
-    for i, (src, dst) in enumerate(((ci_hbm, ci_f), (gi_hbm, gi_f))):
-        halos.append(remote(src.at[pl.ds(edge, HALO)], dst.at[core, pl.ds(0, HALO)],
-                            h_send.at[0, i], h_recv.at[core, i], {"sp": nxt, "tp": jnp.int32(0)}))
-        halos.append(remote(src.at[pl.ds(0, HALO)], dst.at[core, pl.ds(far, HALO)],
-                            h_send.at[1, i], h_recv.at[core, i], {"sp": prv, "tp": jnp.int32(1)}))
-    notes = [
-        remote(docs_hbm, docs.at[1], d_send.at[0], d_recv.at[0], {"sp": nxt, "tp": core}),
-        remote(docs_hbm, docs.at[2], d_send.at[1], d_recv.at[1], {"sp": prv, "tp": core}),
+    to_next = [
+        remote(raw.at[i, pl.ds(edge, HALO)], frames.at[i, core, pl.ds(0, HALO)],
+               h_send.at[0], h_recv.at[0], {"sp": nxt, "tp": jnp.int32(0)}) for i in range(2)]
+    to_prev = [
+        remote(raw.at[i, pl.ds(0, HALO)], frames.at[i, core, pl.ds(far, HALO)],
+               h_send.at[1], h_recv.at[0], {"sp": prv, "tp": jnp.int32(1)}) for i in range(2)]
+    halo_part = frames.at[:, core, pl.ds(0, HALO)]
+    docs_next = remote(docs.at[0], docs.at[1], d_send.at[0], d_recv.at[0], {"sp": nxt, "tp": core})
+    docs_prev = remote(docs.at[0], docs.at[2], d_send.at[0], d_recv.at[0], {"sp": prv, "tp": core})
+    first_half = core == 0
+    inside = (first_half & has_prv) | (jnp.logical_not(first_half) & has_nxt)
+    swaps = [
+        remote(raw.at[i, pl.ds(theirs, span)], frames.at[i, core, pl.ds(their_at, span)],
+               e_send.at[0], e_recv.at[0], partner) for i in range(2)
+    ] + [
+        remote(raw.at[2, pl.ds(pl.multiple_of(other * block, HALO), block)], go_f.at[core],
+               e_send.at[1], e_recv.at[1], partner),
+        remote(taps_hbm, taps_f.at[core], e_send.at[2], e_recv.at[2], partner),
     ]
-    for i, (src, dst) in enumerate(((ci_hbm, ci_f), (gi_hbm, gi_f))):
-        swaps.append(remote(src.at[pl.ds(theirs, span)], dst.at[core, pl.ds(their_at, span)],
-                            e_send.at[i], e_recv.at[i], partner))
-    swaps.append(remote(go_hbm.at[pl.ds(pl.multiple_of(other * block, HALO), block)], go_f.at[core],
-                        e_send.at[2], e_recv.at[2], partner))
-    swaps.append(remote(taps_hbm, taps_f.at[core], e_send.at[3], e_recv.at[3], partner))
-    for copy in halos + notes + swaps:
+    their_frames = frames.at[:, core, pl.ds(their_at, span)]
+    swap_waits = [remote(their_frames, their_frames, e_send.at[0], e_recv.at[0], partner)] + swaps[2:]
+    stage_wait.wait()
+    papers.wait()
+    for copies, there in ((to_next, has_nxt), (to_prev, has_prv)):
+        @pl.when(there)
+        def _():
+            for copy in copies:
+                copy.start()
+
+    @pl.when(first_half & has_nxt)
+    def _():
+        docs_next.start()
+
+    @pl.when(jnp.logical_not(first_half) & has_prv)
+    def _():
+        docs_prev.start()
+
+    for copy in swaps:
         copy.start()
+    project.start()
     lists = []
     for k in range(1, nz):
         to = at_z(lax.rem(z + k, nz))
-        lists.append(remote(routes_hbm, rbuf.at[z], rt_send.at[k, 0], rt_recv.at[k, 0], to))
-        lists.append(remote(rw_hbm, wbuf.at[z], rt_send.at[k, 1], rt_recv.at[k, 1], to))
+        lists.append(remote(routes_hbm, rbuf.at[z], rt_send.at[0], rt_recv.at[0], to))
+        lists.append(remote(rw_hbm, wbuf.at[z], rt_send.at[0], rt_recv.at[0], to))
     for i in range(1, n_plane):
         to = in_plane(lax.rem(p + i, n_plane))
-        lists.append(remote(routes_hbm, rbuf2.at[p], rt2_send.at[i, 0], rt2_recv.at[i, 0], to))
-        lists.append(remote(rw_hbm, wbuf2.at[p], rt2_send.at[i, 1], rt2_recv.at[i, 1], to))
+        lists.append(remote(routes_hbm, rbuf2.at[p], rt_send.at[1], rt_recv.at[1], to))
+        lists.append(remote(rw_hbm, wbuf2.at[p], rt_send.at[1], rt_recv.at[1], to))
     for copy in lists:
         copy.start()
+    list_waits = [
+        remote(lists_of(n - 1), lists_of(n - 1), rt_send.at[i], rt_recv.at[i], partner)
+        for i, n in enumerate((nz, n_plane))
+    ]
 
     lane = lax.broadcasted_iota(jnp.int32, (block, block), 1)
     sub = lax.broadcasted_iota(jnp.int32, (block, block), 0)
@@ -193,21 +234,40 @@
 
         slots(rbuf2[q], wbuf2[q], group // n_core * peers + p * n_core + lax.rem(group, n_core), put)
 
-    for load in tables:
+    tables_wait.wait()
+    line_slots(0)
+
+    for load in front_waits:
         load.wait()
-    line_slots(0)
-
-    for load in front:
-        load.wait()
-    for copy in notes + swaps:
+    for copy in swap_waits:
         copy.wait_recv()
-    for h in range(n_core):
-        for i, dst in enumerate((ci_f, gi_f)):
-            here = dst.at[h, pl.ds(pl.multiple_of(core * far, HALO), HALO)]
-            remote(here, here, h_send.at[0, i], h_recv.at[h, i], partner).wait_recv()
+
+    halo_at = pl.ds(pl.multiple_of(core * far, HALO), HALO)
+
+    @pl.when(inside)
+    def _():
+        docs_next.wait_recv()
+        here = frames.at[:, :, halo_at]
+        remote(here, here, h_send.at[0], h_recv.at[0], partner).wait_recv()
+
+    @pl.when(jnp.logical_not(inside))
+    def _():
+        for h in range(n_core):
+            for i in range(2):
+                frames[i, h, halo_at, :] = jnp.zeros((HALO, half), BF)
+
+    @pl.when(jnp.logical_not(first_half & has_prv))
+    def _():
+        docs[1] = docs[0]
+
+    @pl.when(first_half | jnp.logical_not(has_nxt))
+    def _():
+        docs[2] = docs[0]
+
+    for load in weights:
+        load.start()
 
     own, before_docs, after_docs = docs[0], docs[1], docs[2]
-    first_half = core == 0
     wide = (8, block)
 
     def row(x):
@@ -228,7 +288,7 @@
     keep_before, keep_after = marks[:, 0:1], marks[:, 1:2]
 
     for h in range(n_core):
-        prod[...] = gi_f[h].astype(F32) * ci_f[h].astype(F32)
+        prod[...] = frames[1, h].astype(F32) * frames[0, h].astype(F32)
         conv = (
             taps_f[h, 0:1, :] * (prod[HALO - 1:HALO - 1 + block, :] * keep_before)
             + taps_f[h, 1:2, :] * prod[HALO:HALO + block, :]
@@ -248,17 +308,17 @@
     scale = lax.rsqrt(jnp.sum(square, axis=1, keepdims=True) / width + 1e-05)
 
     def chunk(q):
-        return pl.ds(pl.multiple_of(q * col, col), col)
+        return pl.ds(*cuts[q])
 
     def z_up(h, q):
         b = z - h
         piece = zbuf.at[b, :, chunk(q)]
-        return remote(piece, piece, zu_send.at[h, q], z_recv.at[b, q], at_z(z + 1))
+        return remote(piece, piece, z_send.at[0], z_recv.at[b, q], at_z(z + 1))
 
     def z_down(h, q):
         b = z + h
         piece = zbuf.at[b, :, chunk(q)]
-        return remote(piece, piece, zd_send.at[h, q], z_recv.at[b, q], at_z(z - 1))
+        return remote(piece, piece, z_send.at[0], z_recv.at[b, q], at_z(z - 1))
 
     def normed(cols):
         return (hidden[:, cols] * scale * gain[:, cols]).astype(BF)
@@ -266,14 +326,13 @@
     side = slice(main, width)
     pslab[p] = normed(side)
     s_copies = [
-        remote(pslab.at[p], pslab.at[p], s_send.at[i], s_recv.at[p], in_plane(lax.rem(p + i, n_plane)))
+        remote(pslab.at[p], pslab.at[p], s_send.at[0], s_recv.at[0], in_plane(lax.rem(p + i, n_plane)))
         for i in range(1, n_plane)
     ]
     for copy in s_copies:
         copy.start()
     for q in range(nc):
-        cols = slice(q * col, (q + 1) * col)
-        zbuf[z, :, cols] = normed(cols)
+        zbuf[z, :, chunk(q)] = normed(chunk(q))
 
     for q in range(nc):
         @pl.when(z < nz - 1)
@@ -288,7 +347,7 @@
         @pl.when(z >= h)
         def _():
             piece = zbuf.at[z - h, :, chunk(q)]
-            remote(piece, piece, zu_send.at[h, q], z_recv.at[z - h, q], at_z(z)).wait_recv()
+            remote(piece, piece, z_send.at[0], z_recv.at[z - h, q], at_z(z)).wait_recv()
 
             @pl.when(z < nz - 1)
             def _():
@@ -297,7 +356,7 @@
         @pl.when(z + h < nz)
         def _():
             piece = zbuf.at[z + h, :, chunk(q)]
-            remote(piece, piece, zd_send.at[h, q], z_recv.at[z + h, q], at_z(z)).wait_recv()
+            remote(piece, piece, z_send.at[0], z_recv.at[z + h, q], at_z(z)).wait_recv()
 
             @pl.when(z > 0)
             def _():
@@ -312,31 +371,30 @@
         b = ordered(k)
         return remote(
             outgoing.at[k, pl.ds((j - 1) * cap, cap), chunk(q)], arrived.at[b, pl.ds(my_seat, cap), chunk(q)],
-            a_send.at[b, q], a_recv.at[b, q], plane_peer(j))
-
-    def a_all(k, q):
-        b = ordered(k)
-        return remote(outgoing.at[k, :, chunk(q)], arrived.at[b, pl.ds(cap, rows - cap), chunk(q)],
-                      a_send.at[b, q], a_recv.at[b, q], plane_peer(1))
+            a_send.at[0], a_recv.at[b], plane_peer(j))
+
+    def a_all(k):
+        b = ordered(k)
+        return remote(outgoing.at[k], arrived.at[b, pl.ds(cap, rows - cap), pl.ds(0, main)],
+                      a_send.at[0], a_recv.at[b], plane_peer(1))
 
     def r_copy(k, j, q):
         b = ordered(k)
         seat = seat_of(lax.rem(rank + peers - j, peers))
         return remote(
             arrived.at[b, pl.ds(seat, cap), chunk(q)], returned.at[b, pl.ds(j * cap, cap), chunk(q)],
-            r_send.at[b, q], r_recv.at[b, q], plane_peer(peers - j))
+            r_send.at[0], r_recv.at[b, q], plane_peer(peers - j))
 
     def r_all(k, q):
         b = ordered(k)
         return remote(
             arrived.at[b, pl.ds(cap, rows - cap), chunk(q)], returned.at[b, pl.ds(cap, rows - cap), chunk(q)],
-            r_send.at[b, q], r_recv.at[b, q], plane_peer(1))
+            r_send.at[0], r_recv.at[b, q], plane_peer(1))
 
     def dispatch(k):
         b = ordered(k)
 
-        @pl.loop(0, nc)
-        def _(q):
+        for q in range(nc):
             if k:
                 pump(k, q)
             cols = chunk(q)
@@ -353,26 +411,34 @@
 
     def v_copy(b, c):
         return remote(
-            outgoing2.at[b, c], arrived.at[z, pl.ds(my_lot, lot), side_ref],
-            v_send.at[b, c], v_recv.at[z, core], {"sp": b * n_plane + p, "tp": c})
-
-    def v_wait(b, c):
-        piece = arrived.at[b, pl.ds(pl.multiple_of(c * lot, HALO), lot), side_ref]
-        remote(piece, piece, v_send.at[b, c], v_recv.at[b, c], partner).wait_recv()
+            outgoing2.at[b * n_core + c], arrived.at[z, pl.ds(my_lot, lot), side_ref],
+            v_send.at[0], v_recv.at[z], {"sp": b * n_plane + p, "tp": c})
+
+    def v_wait(b, count):
+        piece = arrived.at[b, pl.ds(0, count * lot), side_ref]
+        remote(piece, piece, v_send.at[0], v_recv.at[b], partner).wait_recv()
+
+    def rest(ref):
+        return ref.at[pl.ds(0, ref.shape[0] - 1)]
+
+    def all_of(ref, send, recv):
+        return remote(ref, ref, send, recv, partner)
+
+    s_all = all_of(rest(pslab), s_send.at[0], s_recv.at[0])
+    v_all = all_of(rest(outgoing2), v_send.at[0], v_recv.at[0])
+    w_all = all_of(rest(returned2), w_send.at[0], w_recv.at[0])
+    f_all = all_of(rest(partial2), f_send.at[0], f_recv.at[0])
 
     def side_pick():
+        s_all.wait_recv()
         for q in range(n_plane):
-            @pl.when(p != q)
-            def _():
-                remote(pslab.at[q], pslab.at[q], s_send.at[1], s_recv.at[q], partner).wait_recv()
-
             plane_slots(q)
             picked = dot(select2[q], pslab[q]).astype(BF)
             for b in range(nz):
                 for c in range(n_core):
                     at = (b * n_core + c) * cap
-                    outgoing2[b, c, q * cap:(q + 1) * cap, :] = picked[at:at + cap]
-        arrived[z, pl.ds(my_lot, lot), side] = outgoing2[z, core]
+                    outgoing2[b * n_core + c, q * cap:(q + 1) * cap, :] = picked[at:at + cap]
+        arrived[z, pl.ds(my_lot, lot), side] = outgoing2[z * n_core + core]
         v_copy(z, other).start()
 
     def side_send(h):
@@ -388,22 +454,17 @@
 
     def w_copy(b, c):
         piece = arrived.at[b, pl.ds(pl.multiple_of(c * lot, HALO), lot), side_ref]
-        return remote(piece, returned2.at[z, core], w_send.at[b, c], w_recv.at[z, core],
+        return remote(piece, returned2.at[z * n_core + core], w_send.at[0], w_recv.at[0],
                       {"sp": b * n_plane + p, "tp": c})
 
     def f_copy(q):
-        return remote(partial2.at[q], summed2.at[p], f_send.at[q], f_recv.at[p], in_plane(q))
+        return remote(partial2.at[q], summed2.at[p], f_send.at[0], f_recv.at[0], in_plane(q))
 
     def side_combine():
-        for b in range(nz):
-            for c in range(n_core):
-                @pl.when((z != b) | (core != c))
-                def _():
-                    piece = returned2.at[b, c]
-                    remote(piece, piece, w_send.at[b, c], w_recv.at[b, c], partner).wait_recv()
+        w_all.wait_recv()
         for q in range(n_plane):
             results = jnp.concatenate(
-                [returned2[b, c, q * cap:(q + 1) * cap, :] for b in range(nz) for c in range(n_core)], axis=0)
+                [returned2[b, q * cap:(q + 1) * cap, :] for b in range(nz * n_core)], axis=0)
             total = dot(spread2[q], results)
 
             @pl.when(p == q)
@@ -422,14 +483,11 @@
         if k == 0:
             for load in weights:
                 load.wait()
-            v_wait(z, other)
+            v_wait(z, n_core - 1)
         else:
-            for c in range(n_core):
-                v_wait(b, c)
-
-        @pl.loop(0, nc)
-        def _(q):
-            a_all(k, q).wait_recv()
+            v_wait(b, n_core)
+
+        a_all(k).wait_recv()
 
         @pl.loop(0, ff // fcol)
         def _(i):
@@ -440,14 +498,13 @@
 
         arrived[b, :, side] = dot(act[...], wd[:, side]).astype(BF)
         if k == 0:
-            returned2[z, core] = arrived[z, pl.ds(my_lot, lot), side]
+            returned2[z * n_core + core] = arrived[z, pl.ds(my_lot, lot), side]
             w_copy(z, other).start()
         else:
             for c in range(n_core):
                 w_copy(b, c).start()
 
-        @pl.loop(0, nc)
-        def _(q):
+        for q in range(nc):
             cols = chunk(q)
             arrived[b, :, cols] = dot(act[...], wd[:, cols]).astype(BF)
             returned[b, 0:cap, cols] = arrived[b, pl.ds(my_seat, cap), cols]
@@ -466,17 +523,16 @@
         down = b < z
         seat = jnp.where(down & (b == z - 1), nz, b)
         return remote(partial.at[k - 1, :, chunk(q)], chain.at[seat, :, chunk(q)],
-                      p_send.at[k, q], p_recv.at[seat, q], at_z(jnp.where(down, z - 1, z + 1)))
+                      p_send.at[0], p_recv.at[seat, q], at_z(jnp.where(down, z - 1, z + 1)))
 
     def p_wait(seat, q):
         piece = chain.at[seat, :, chunk(q)]
-        remote(piece, piece, p_send.at[0, q], p_recv.at[seat, q], at_z(z)).wait_recv()
+        remote(piece, piece, p_send.at[0], p_recv.at[seat, q], at_z(z)).wait_recv()
 
     def combine(k):
         b = ordered(k)
 
-        @pl.loop(0, nc)
-        def _(q):
+        for q in range(nc):
             cols = chunk(q)
             r_all(k, q).wait_recv()
             total = dot(spread[k], returned[b, :, cols])
@@ -494,8 +550,12 @@
 
                 p_copy(k, q).start()
 
+    def give_all(k, low, high):
+        for q in range(low, high):
+            give(k, q)
+
     dispatch(0)
-    for copy in lists:
+    for copy in list_waits:
         copy.wait_recv()
     side_pick()
     for k in range(1, nz):
@@ -504,31 +564,23 @@
         side_send(k)
         if k < nz - 1:
             expert(k - 1)
-
-    def give_all(k, low, high):
-        @pl.loop(low, high)
-        def _(q):
-            give(k, q)
-
-    give_all(0, 0, nc // 2)
+    give_all(0, 0, nc)
     expert(nz - 2)
     expert(nz - 1)
     for k in range(nz - 2, 0, -1):
         give_all(k, 0, nc)
     combine(nz - 1)
     side_combine()
-    give_all(0, nc // 2, nc)
     for k in range(nz - 2, -1, -1):
         combine(k)
+    f_all.wait_recv()
     for q in range(n_plane):
         @pl.when(p != q)
         def _():
-            remote(summed2.at[q], summed2.at[q], f_send.at[q], f_recv.at[q], partner).wait_recv()
             hidden[:, side] = hidden[:, side] + summed2[q].astype(F32)
     out_ref[:, side] = hidden[:, side].astype(BF)
 
-    @pl.loop(0, nc)
-    def _(q):
+    for q in range(nc):
         cols = chunk(q)
 
         @pl.when(z > 0)
@@ -543,34 +595,30 @@
 
         out_ref[:, cols] = hidden[:, cols].astype(BF)
 
-    for copy in halos + notes + swaps + lists + s_copies:
+    for i, there in enumerate((has_nxt, has_prv)):
+        @pl.when(there)
+        def _():
+            remote(halo_part, halo_part, h_send.at[i], h_recv.at[0], partner).wait_send()
+
+    @pl.when((first_half & has_nxt) | (jnp.logical_not(first_half) & has_prv))
+    def _():
+        docs_next.wait_send()
+
+    for copy in swap_waits + list_waits + [s_all, v_all, w_all, f_all]:
         copy.wait_send()
-    for b in range(nz):
-        for c in range(n_core):
-            @pl.when((z != b) | (core != c))
-            def _():
-                v_copy(jnp.int32(b), jnp.int32(c)).wait_send()
-                w_copy(jnp.int32(b), jnp.int32(c)).wait_send()
-    for q in range(n_plane):
-        @pl.when(p != q)
-        def _():
-            f_copy(jnp.int32(q)).wait_send()
-
-    @pl.loop(0, nc)
-    def _(q):
-        for h in range(nz):
-            @pl.when((z >= h) & (z < nz - 1))
-            def _():
-                z_up(h, q).wait_send()
-
-            @pl.when((z + h < nz) & (z > 0))
-            def _():
-                z_down(h, q).wait_send()
-        for k in range(nz):
-            a_all(k, q).wait_send()
-            r_all(k, q).wait_send()
-            if k:
-                p_copy(k, q).wait_send()
+    middle = (z > 0) & (z < nz - 1)
+
+    @pl.when(middle)
+    def _():
+        remote(chain, chain, z_send.at[0], z_recv.at[0, 0], partner).wait_send()
+
+    @pl.when(jnp.logical_not(middle))
+    def _():
+        remote(chain.at[0], chain.at[0], z_send.at[0], z_recv.at[0, 0], partner).wait_send()
+
+    remote(outgoing, outgoing, a_send.at[0], a_recv.at[0], partner).wait_send()
+    remote(outgoing, outgoing, r_send.at[0], r_recv.at[0, 0], partner).wait_send()
+    remote(partial, partial, p_send.at[0], p_recv.at[0, 0], partner).wait_send()
 
 
 def layer(n_seq, nz, n_plane, n_core, cap, *args):
@@ -584,14 +632,16 @@
     frame = block + 2 * HALO
     slab = SLAB if width > 2 * SLAB else 128
     main = width - slab
-    col = tile_of(main, COL)
-    nc = main // col
+    parts = main // 128
+    nc = min(CHUNKS, parts)
+    edges = [-(-parts * i // nc) * 128 for i in range(nc + 1)]
+    cuts = [(a, b - a) for a, b in zip(edges, edges[1:])]
     lot = n_plane * cap
     hbm = pl.BlockSpec(memory_space=pl.ANY)
     vmem = pl.BlockSpec(memory_space=pltpu.VMEM)
     dma = pltpu.SemaphoreType.DMA
     return pl.pallas_call(
-        functools.partial(layer_kernel, n_seq, nz, n_plane, n_core, cap, col, slab),
+        functools.partial(layer_kernel, n_seq, nz, n_plane, n_core, cap, cuts, slab),
         out_shape=jax.ShapeDtypeStruct((block, width), BF),
         in_specs=[hbm] * len(args),
         out_specs=vmem,
@@ -600,8 +650,8 @@
             pltpu.VMEM((width, ff), BF),
             pltpu.VMEM((ff, width), BF),
             pltpu.VMEM((channels, width), BF),
-            pltpu.VMEM((n_core, frame, half), BF),
-            pltpu.VMEM((n_core, frame, half), BF),
+            pltpu.VMEM((3, tok, half), BF),
+            pltpu.VMEM((2, n_core, frame, half), BF),
             pltpu.VMEM((n_core, block, half), BF),
             pltpu.VMEM((n_core,) + args[3].shape, F32),
             pltpu.VMEM((3, n_core, block), jnp.int32),
@@ -626,18 +676,15 @@
             pltpu.VMEM((n_plane, nz * n_core * cap, block), BF),
             pltpu.VMEM((n_plane, block, nz * n_core * cap), BF),
             pltpu.VMEM((n_plane, block, slab), BF),
-            pltpu.VMEM((nz, n_core, lot, slab), BF),
-            pltpu.VMEM((nz, n_core, lot, slab), BF),
+            pltpu.VMEM((nz * n_core, lot, slab), BF),
+            pltpu.VMEM((nz * n_core, lot, slab), BF),
             pltpu.VMEM((n_plane, block, slab), BF),
             pltpu.VMEM((n_plane, block, slab), BF),
-            dma((15,)), dma((4,)), dma((4,)), dma((2, 2)), dma((n_core, 2)),
-            dma((2,)), dma((2,)), dma((nz, 2)), dma((nz, 2)),
-            dma((nz, nc)), dma((nz, nc)), dma((nz, nc)),
-            dma((nz, nc)), dma((nz, nc)), dma((nz, nc)), dma((nz, nc)),
-            dma((nz, nc)), dma((nz + 1, nc)),
-            dma((n_plane, 2)), dma((n_plane, 2)), dma((n_plane,)), dma((n_plane,)),
-            dma((nz, n_core)), dma((nz, n_core)), dma((nz, n_core)), dma((nz, n_core)),
-            dma((n_plane,)), dma((n_plane,)),
+            dma((12,)), dma((3,)), dma((3,)), dma((2,)), dma((1,)),
+            dma((1,)), dma((1,)), dma((2,)), dma((2,)),
+            dma((1,)), dma((nz, nc)), dma((1,)), dma((nz,)), dma((1,)), dma((nz, nc)),
+            dma((1,)), dma((nz + 1, nc)),
+            dma((1,)), dma((1,)), dma((1,)), dma((nz,)), dma((1,)), dma((1,)), dma((1,)), dma((1,)),
         ],
         compiler_params=pltpu.CompilerParams(
             collective_id=0, has_side_effects=True, vmem_limit_bytes=62 * 2**20),

time: 104 us -> 101 us (0.971)
  Pallas kernels: 102 us -> 97.9 us
    pallas_call x1, Pallas kernels: 102 us -> 97.9 us  [layer(): pl.pallas_call(functools.partial(layer_kernel, n_seq, nz, n_plane, n_core...]
where the time goes in v4:
time: 101 us; the launch traced here: 99.8 us
  Pallas kernels  97.9 us (97%)
  local copies, waits for them, and re-layouts  1.88 us (2%)
    pallas_call x1, Pallas kernels, layer(): pl.pallas_call(functools.partial(layer_kernel, n_seq, nz, n_plane, n_core...  97.9 us

profile of v4, /device:TPU:0, one launch (start us, length us, event | category | flops | bytes accessed | tf_op | source)
XLA Modules:
  0.0 99.8 jit_solution(9219361567910417259)
XLA Ops:
  0.0 97.9 %mixer_experts.1 = bf16[128,2048]{1,0:T(8,128)(2,1)} custom-call(bf16[256,512]{1,0:T(8,128)(2,1)} %ci_hbm.1, bf16[256,512]{1,0:T(8,128)(2,1)} %go_hbm.1, bf16[256,512]{1,0:T(8,128)(2,1)} %gi_hbm.1, f32[3,512]{1,0:T(4,128)} %taps_hbm.1, s32[2,128]{1,0:T(2,128)} %bitcast.13, bf16[1024,2048]{1,0:T(8,128)(2,1)} %wp_hbm.1, bf16[128,2048]{1,0:T(8,128)(2,1)} %stream_hbm.1, ...), custom_call_target="tpu_custom_call" | custom-call | tf_op jit(solution)/shard_map/mixer_experts/pallas_call | solution.py:643
  97.9 1.9 %copy.15 = bf16[128,2048]{1,0:T(8,128)(2,1)} copy(bf16[128,2048]{1,0:T(8,128)(2,1)} %mixer_experts.1) | data formatting | bytes 1048576

commit v5 on v4

--- a/solution.py
+++ b/solution.py
@@ -10,8 +10,8 @@
 
 MESH = pl.DeviceIdType.MESH
 HALO = 16
-SLAB = 384
-CHUNKS = 2
+SLAB = 512
+CHUNKS = 3
 BF = jnp.bfloat16
 F32 = jnp.float32
 
@@ -557,14 +557,17 @@
     dispatch(0)
     for copy in list_waits:
         copy.wait_recv()
-    side_pick()
     for k in range(1, nz):
         line_slots(k)
+        if k == nz - 1:
+            give_all(0, 0, nc // 2)
         dispatch(k)
+        if k == 1:
+            side_pick()
         side_send(k)
         if k < nz - 1:
             expert(k - 1)
-    give_all(0, 0, nc)
+    give_all(0, nc // 2, nc)
     expert(nz - 2)
     expert(nz - 1)
     for k in range(nz - 2, 0, -1):

time: 101 us -> 96.1 us (0.951); the launches traced: 99.8 us -> 95.9 us
  Pallas kernels: 97.9 us -> 94 us
    pallas_call x1, Pallas kernels: 97.9 us -> 94 us  [layer(): pl.pallas_call(functools.partial(layer_kernel, n_seq, nz, n_plane, n_core...]
where the time goes in v5:
time: 96.1 us; the launch traced here: 95.9 us
  Pallas kernels  94 us (98%)
  local copies, waits for them, and re-layouts  1.88 us (2%)
    pallas_call x1, Pallas kernels, layer(): pl.pallas_call(functools.partial(layer_kernel, n_seq, nz, n_plane, n_core...  94 us

profile of v5, /device:TPU:0, one launch (start us, length us, event | category | flops | bytes accessed | tf_op | source)
XLA Modules:
  0.0 95.9 jit_solution(11710295621879587392)
XLA Ops:
  0.0 94.0 %mixer_experts.1 = bf16[128,2048]{1,0:T(8,128)(2,1)} custom-call(bf16[256,512]{1,0:T(8,128)(2,1)} %ci_hbm.1, bf16[256,512]{1,0:T(8,128)(2,1)} %go_hbm.1, bf16[256,512]{1,0:T(8,128)(2,1)} %gi_hbm.1, f32[3,512]{1,0:T(4,128)} %taps_hbm.1, s32[2,128]{1,0:T(2,128)} %bitcast.13, bf16[1024,2048]{1,0:T(8,128)(2,1)} %wp_hbm.1, bf16[128,2048]{1,0:T(8,128)(2,1)} %stream_hbm.1, ...), custom_call_target="tpu_custom_call" | custom-call | tf_op jit(solution)/shard_map/mixer_experts/pallas_call | solution.py:646
  94.0 1.9 %copy.15 = bf16[128,2048]{1,0:T(8,128)(2,1)} copy(bf16[128,2048]{1,0:T(8,128)(2,1)} %mixer_experts.1) | data formatting | bytes 1048576

commit v6 on v5

--- a/solution.py
+++ b/solution.py
@@ -36,7 +36,7 @@
     out_ref,
     wg, wu, wd, wp, raw, frames, go_f, taps_f, docs, prod, mixed, stream, gain, hidden,
     rbuf, wbuf, select, spread, zbuf, outgoing, arrived, act, returned, partial, chain,
-    rbuf2, wbuf2, select2, spread2, pslab, outgoing2, returned2, partial2, summed2,
+    early, rbuf2, wbuf2, select2, spread2, pslab, outgoing2, returned2, partial2, summed2,
     l_sem, e_send, e_recv, h_send, h_recv, d_send, d_recv, rt_send, rt_recv,
     z_send, z_recv, a_send, a_recv, r_send, r_recv, p_send, p_recv,
     s_send, s_recv, v_send, v_recv, w_send, w_recv, f_send, f_recv,
@@ -483,17 +483,21 @@
         if k == 0:
             for load in weights:
                 load.wait()
-            v_wait(z, n_core - 1)
-        else:
-            v_wait(b, n_core)
-
         a_all(k).wait_recv()
 
         @pl.loop(0, ff // fcol)
         def _(i):
             cols = pl.ds(pl.multiple_of(i * fcol, fcol), fcol)
-            gate = jnp.minimum(dot(arrived[b], wg[:, cols]), 7.0)
-            upper = jnp.clip(dot(arrived[b], wu[:, cols]), -7.0, 7.0)
+            early[0, :, cols] = dot(arrived[b, :, 0:main], wg[0:main, cols])
+            early[1, :, cols] = dot(arrived[b, :, 0:main], wu[0:main, cols])
+
+        v_wait(b, n_core if k else n_core - 1)
+
+        @pl.loop(0, ff // fcol)
+        def _(i):
+            cols = pl.ds(pl.multiple_of(i * fcol, fcol), fcol)
+            gate = jnp.minimum(early[0, :, cols] + dot(arrived[b, :, side], wg[side, cols]), 7.0)
+            upper = jnp.clip(early[1, :, cols] + dot(arrived[b, :, side], wu[side, cols]), -7.0, 7.0)
             act[:, cols] = ((upper + 1.0) * gate * jax.nn.sigmoid(1.702 * gate)).astype(BF)
 
         arrived[b, :, side] = dot(act[...], wd[:, side]).astype(BF)
@@ -674,6 +678,7 @@
             pltpu.VMEM((nz, rows, main), BF),
             pltpu.VMEM((nz - 1, block, main), BF),
             pltpu.VMEM((nz + 1, block, main), BF),
+            pltpu.VMEM((2, rows, ff), F32),
             pltpu.VMEM((n_plane, topk, block), jnp.int32),
             pltpu.VMEM((n_plane, topk, block), F32),
             pltpu.VMEM((n_plane, nz * n_core * cap, block), BF),

time: 96.1 us -> 95.1 us (0.990)
  Pallas kernels: 94 us -> 93 us
where the time goes in v6:
time: 95.1 us; the launch traced here: 94.9 us
  Pallas kernels  93 us (98%)
  local copies, waits for them, and re-layouts  1.88 us (2%)
    pallas_call x1, Pallas kernels, layer(): pl.pallas_call(functools.partial(layer_kernel, n_seq, nz, n_plane, n_core...  93 us

profile of v6, /device:TPU:0, one launch (start us, length us, event | category | flops | bytes accessed | tf_op | source)
XLA Modules:
  0.0 94.9 jit_solution(7815208590342999883)
XLA Ops:
  0.0 93.0 %mixer_experts.1 = bf16[128,2048]{1,0:T(8,128)(2,1)} custom-call(bf16[256,512]{1,0:T(8,128)(2,1)} %ci_hbm.1, bf16[256,512]{1,0:T(8,128)(2,1)} %go_hbm.1, bf16[256,512]{1,0:T(8,128)(2,1)} %gi_hbm.1, f32[3,512]{1,0:T(4,128)} %taps_hbm.1, s32[2,128]{1,0:T(2,128)} %bitcast.13, bf16[1024,2048]{1,0:T(8,128)(2,1)} %wp_hbm.1, bf16[128,2048]{1,0:T(8,128)(2,1)} %stream_hbm.1, ...), custom_call_target="tpu_custom_call" | custom-call | tf_op jit(solution)/shard_map/mixer_experts/pallas_call | solution.py:650
  93.1 1.9 %copy.15 = bf16[128,2048]{1,0:T(8,128)(2,1)} copy(bf16[128,2048]{1,0:T(8,128)(2,1)} %mixer_experts.1) | data formatting | bytes 1048576
